TPU v7x, 32 devices: a whole 2x2x4 slice. The times are simulated.
32 devices in a mesh: grp: 2 (over x), ep: 4 (over y, core), tp: 4 (over z).
Axes of the slice: x: 2, y: 2, z: 4, core: 2. Of those that a mesh axis runs over, the one named last changes fastest.
Arguments:
- mixer_in: bfloat16 [4096, 2048], P(('grp', 'ep', 'tp')), parts along dimension 0, may hold values from -600 to 600
- mixer_gain: float32 [2048], replicated, may hold values from 0.1 to 1.9
- w_query: bfloat16 [2048, 1024], P(None, 'tp'), may hold values from -6 to 6
- w_key: bfloat16 [2048, 512], P(None, 'tp'), may hold values from -0.1875 to 0.1875
- w_value: bfloat16 [2048, 512], P(None, 'tp'), may hold values from -0.25 to 0.25
- sink_logit: float32 [16], P('tp'), may hold values from 3 to 9
- moe_in: bfloat16 [4096, 2048], P(('grp', 'ep', 'tp')), parts along dimension 0, may hold values from -600 to 600
- moe_gain: float32 [2048], replicated, may hold values from 0.1 to 1.9
- router: bfloat16 [2048, 16], replicated, may hold values from -0.25 to 0.25
- routes: int32 [4096, 4], P(('grp', 'ep', 'tp')), parts along dimension 0, may hold values from 0 to 15, all different within a row; in each aligned block of 128 rows (0 to 127, 128 to 255, ...) at most 48 rows name the same one
- expert_gate: bfloat16 [16, 2048, 512], P(('ep', 'tp')), may hold values from -0.125 to 0.125
- expert_up: bfloat16 [16, 2048, 512], P(('ep', 'tp')), may hold values from -0.125 to 0.125
- expert_down: bfloat16 [16, 512, 2048], P(('ep', 'tp')), may hold values from -0.25 to 0.25
- shared_gate: bfloat16 [2048, 512], P(None, 'tp'), may hold values from -0.125 to 0.125
- shared_up: bfloat16 [2048, 512], P(None, 'tp'), may hold values from -0.125 to 0.125
- shared_down: bfloat16 [512, 2048], P('tp'), may hold values from -0.25 to 0.25
Outputs:
- mixed: bfloat16 [4096, 1024], P(('grp', 'ep'), 'tp'), parts along dimension 0
- moe_out: bfloat16 [4096, 2048], P(('grp', 'ep', 'tp')), parts along dimension 0
There are 2 independent parts, one for each index of `grp`. A program takes and returns all parts, laid end to end along the dimension named above; an argument that names none is the same for every part. Nothing has to cross between parts.
Inputs may be any that keep to these rules, and one draw needn't show every extreme that they name: `routes`: each row names 4 different experts. Within the rows of one device (aligned blocks of 128 rows) no expert is named by more than 48 rows, a bound that some block reaches.
All inputs are finite; a program needn't handle non-finite values.
Results may differ from a plain program's by a relative error of at most 0.012.
Values may be sent and summed in bfloat16 or wider, within the bound.
A program may use at most 128 MiB of HBM per device.

v0:
```python
import functools

import jax
import jax.numpy as jnp
from jax import lax
from jax.experimental import pallas as pl
from jax.experimental.pallas import tpu as pltpu
from jax.sharding import PartitionSpec as P

HEAD_DIM = 64
WINDOW = 128


EPS = 1e-06
THETA = 10000.0
ROUTED_SCALE = 2.5


def extended(block, sides, width):
    for axis, dim in sides:
        count = lax.axis_size(axis)
        forward = [(i, i + 1) for i in range(count - 1)]
        backward = [(target, source) for source, target in forward]
        low = lax.ppermute(
            lax.slice_in_dim(block, block.shape[dim] - width, None, axis=dim), axis, forward
        )
        high = lax.ppermute(lax.slice_in_dim(block, 0, width, axis=dim), axis, backward)
        block = jnp.concatenate([low, block, high], axis=dim)
    return block


def rms_rows(row_block, gain_vector):
    values = row_block.astype(jnp.float32)
    factor = lax.rsqrt(jnp.mean(values * values, axis=-1, keepdims=True) + EPS)
    return (values * factor * gain_vector).astype(jnp.bfloat16)


def rotate(head_rows, positions):
    half_width = head_rows.shape[-1] // 2
    inverse = THETA ** (-(jnp.arange(half_width, dtype=jnp.float32) * 2.0) / head_rows.shape[-1])
    angles = positions.astype(jnp.float32)[:, None] * inverse[None, :]
    cosine_table = jnp.cos(angles)[:, None, :]
    sine_table = jnp.sin(angles)[:, None, :]
    first_half = head_rows[..., :half_width]
    second_half = head_rows[..., half_width:]
    return jnp.concatenate(
        [
            first_half * cosine_table - second_half * sine_table,
            second_half * cosine_table + first_half * sine_table,
        ],
        axis=-1,
    )


def attend(query_rows, stacked, sink_logit, offset, seq_length):
    span_rows, head_count, head_width = query_rows.shape
    kv_local = stacked.shape[1] // (2 * head_width)
    group_size = head_count // kv_local
    key_table = stacked[:, : kv_local * head_width].reshape(-1, kv_local, head_width)
    value_table = stacked[:, kv_local * head_width :].reshape(-1, kv_local, head_width)
    block_rows = 512
    grouped = query_rows.reshape(span_rows, kv_local, group_size, head_width)
    row_ids = jnp.arange(block_rows, dtype=jnp.int32)[:, None]
    col_ids = jnp.arange(block_rows + 2 * WINDOW, dtype=jnp.int32)[None, :]
    sink_table = sink_logit.reshape(kv_local, group_size)[:, :, None, None]

    def one_block(block_index):
        block_start = block_index * block_rows
        query_block = lax.dynamic_slice_in_dim(grouped, block_start, block_rows, 0)
        key_block = lax.dynamic_slice_in_dim(key_table, block_start, block_rows + 2 * WINDOW, 0)
        value_block = lax.dynamic_slice_in_dim(value_table, block_start, block_rows + 2 * WINDOW, 0)
        scores = jnp.einsum(
            "qkgd,ckd->kgqc", query_block, key_block, preferred_element_type=jnp.float32
        ) * head_width ** (-0.5)
        key_pos = offset + block_start - WINDOW + col_ids
        query_pos = offset + block_start + row_ids
        in_window = (
            (jnp.abs(key_pos - query_pos) <= WINDOW) & (key_pos >= 0) & (key_pos < seq_length)
        )
        scores = jnp.where(in_window[None, None], scores, -jnp.inf)
        row_max = jnp.maximum(jnp.max(scores, axis=-1, keepdims=True), sink_table)
        weights = jnp.exp(scores - row_max)
        denominator = jnp.sum(weights, axis=-1, keepdims=True) + jnp.exp(sink_table - row_max)
        probability = (weights / denominator).astype(jnp.bfloat16)
        output = jnp.einsum(
            "kgqc,ckd->qkgd", probability, value_block, preferred_element_type=jnp.float32
        )
        return output.reshape(block_rows, head_count * head_width).astype(jnp.bfloat16)

    blocks_out = lax.map(one_block, jnp.arange(span_rows // block_rows, dtype=jnp.int32))
    return blocks_out.reshape(span_rows, head_count * head_width)


MESH = pl.DeviceIdType.MESH
VMEM_LIMIT = 63 * 2**20
CHUNK = 512


def remote(src, dst, send_sem, recv_sem, device):
    return pltpu.make_async_remote_copy(
        src_ref=src,
        dst_ref=dst,
        send_sem=send_sem,
        recv_sem=recv_sem,
        device_id=device,
        device_id_type=MESH,
    )


def entry_barrier(grp, ep, tp, ep_count, tp_count):
    barrier = pltpu.get_barrier_semaphore()

    @pl.when(tp > 0)
    def _():
        pl.semaphore_signal(barrier, inc=1, device_id=(grp, ep, tp - 1), device_id_type=MESH)

    @pl.when(tp < tp_count - 1)
    def _():
        pl.semaphore_signal(barrier, inc=1, device_id=(grp, ep, tp + 1), device_id_type=MESH)

    for d in range(1, ep_count):
        pl.semaphore_signal(
            barrier, inc=1, device_id=(grp, lax.rem(ep + d, ep_count), tp), device_id_type=MESH
        )

    inner = (tp > 0) & (tp < tp_count - 1)
    pl.semaphore_wait(barrier, ep_count + jnp.where(inner, 1, 0))


def layer_kernel(
    ep_count, tp_count, slots,
    second, first, meta, gate_hbm, up_hbm, down_hbm, sgate, sup, sdown,
    out, gath1,
    gath2, metag, sbuf, disp, back, sides, psend, gate, up, down, hidden, hexp,
    own_sem, w_sem, s2, r2, sm, rm, s1, r1, sd, rd, sb, rb, sp, rs,
):
    grp, ep, tp = lax.axis_index("grp"), lax.axis_index("ep"), lax.axis_index("tp")
    rows, width = second.shape
    experts = meta.shape[0] // 2
    total = ep_count * slots
    entry_barrier(grp, ep, tp, ep_count, tp_count)
    own_copies = [
        pltpu.make_async_copy(second, gath2.at[tp], own_sem.at[0]),
        pltpu.make_async_copy(meta, metag.at[tp], own_sem.at[1]),
        pltpu.make_async_copy(first, gath1.at[tp], own_sem.at[2]),
    ]
    weight_copies = [
        pltpu.make_async_copy(gate_hbm.at[0], gate, w_sem.at[0]),
        pltpu.make_async_copy(up_hbm.at[0], up, w_sem.at[1]),
        pltpu.make_async_copy(down_hbm.at[0], down, w_sem.at[2]),
    ]

    def toward(side):
        return (grp, ep, tp + (1 if side == 0 else -1))

    def exists(side):
        return tp < tp_count - 1 if side == 0 else tp > 0

    def peer(d):
        return (grp, lax.rem(ep + d, ep_count), tp)

    def spans(body, size=CHUNK, extent=width):
        def step(c, carry):
            body(pl.ds(pl.multiple_of(c * size, size), size))
            return carry

        lax.fori_loop(0, extent // size, step, 0)

    def send_second(side, block, own):
        return [
            remote(second if own else gath2.at[block], gath2.at[block], s2.at[side, block], r2.at[block], toward(side)),
            remote(meta if own else metag.at[block], metag.at[block], sm.at[side, block], rm.at[block], toward(side)),
        ]

    def send_first(side, block, own):
        return remote(first if own else gath1.at[block], gath1.at[block], s1.at[side, block], r1.at[block], toward(side))

    def start_own_first(side, step):
        last = tp if side == 0 else tp_count - 1 - tp

        @pl.when(exists(side) & (step == last))
        def _():
            send_first(side, tp, True).start()

    def dispatch_copy(block, d):
        part = pl.ds(d * slots, slots)
        return remote(sbuf.at[block, part], disp.at[block, part], sd.at[block, d], rd.at[block, d], peer(d))

    def return_copy(block, d):
        part = pl.ds(d * slots, slots)
        return remote(sbuf.at[block, part], back.at[block, part], sb.at[block, d], rb.at[block, d], peer(ep_count - d))

    parts = width // CHUNK

    def part_span(part):
        return pl.ds(pl.multiple_of(part * CHUNK, CHUNK), CHUNK)

    def pass_on(side, block, part):
        span = part_span(part)
        return remote(
            psend.at[block, :, span], sides.at[side, block, :, span],
            sp.at[block, part], rs.at[side, block, part], toward(side),
        )

    def places_of(block, d):
        expert = lax.rem(ep + d, ep_count) * tp_count + tp
        slot_ids = lax.broadcasted_iota(jnp.int32, (slots, rows), 0).astype(jnp.float32)
        return slot_ids == metag[block, pl.ds(expert, 1), :], expert

    def process(block):
        picks = [jnp.where(places_of(block, d)[0], 1.0, 0.0) for d in range(ep_count)]
        pick = jnp.concatenate(picks, axis=0).astype(jnp.bfloat16)

        def columns(span):
            picked = jnp.dot(pick, gath2[block, :, span], preferred_element_type=jnp.float32).astype(jnp.bfloat16)
            disp[block, 0:slots, span] = picked[0:slots]
            sbuf[block, slots:total, span] = picked[slots:total]

        spans(columns)
        for d in range(1, ep_count):
            dispatch_copy(block, d).start()

    def shared_hidden(block):
        values = gath2[block]
        gated = jnp.dot(values, sgate[...], preferred_element_type=jnp.float32)
        lifted = jnp.dot(values, sup[...], preferred_element_type=jnp.float32)
        hidden[block] = (jax.nn.silu(gated) * lifted).astype(jnp.bfloat16)

    def expert(block):
        for d in range(1, ep_count):
            dispatch_copy(block, d).wait()

        def units(span):
            values = disp[block]
            gated = jnp.dot(values, gate[:, span], preferred_element_type=jnp.float32)
            lifted = jnp.dot(values, up[:, span], preferred_element_type=jnp.float32)
            hexp[:, span] = (jax.nn.silu(gated) * lifted).astype(jnp.bfloat16)

        spans(units, 256, gate.shape[1])

        def columns(span):
            result = jnp.dot(hexp[...], down[:, span], preferred_element_type=jnp.float32).astype(jnp.bfloat16)
            back[block, 0:slots, span] = result[0:slots]
            sbuf[block, slots:total, span] = result[slots:total]

        spans(columns)

    def give_back(block):
        for d in range(1, ep_count):
            return_copy(block, d).start()

    def experts_at(distance):
        def one(side, carry):
            block = tp + (2 * side - 1) * distance

            @pl.when((block >= 0) & (block < tp_count) & ((distance > 0) | (side == 0)))
            def _():
                expert(block)

                @pl.when(block != tp)
                def _():
                    give_back(block)

            return carry

        lax.fori_loop(0, 2, one, 0)

    for side in range(2):

        @pl.when(exists(side))
        def _():
            for copy in send_second(side, tp, True):
                copy.start()

        start_own_first(side, 0)
    for copy in own_copies + weight_copies:
        copy.start()

    @pl.when(tp == 0)
    def _():
        sides[0] = jnp.zeros(sides.shape[1:], sides.dtype)

    @pl.when(tp == tp_count - 1)
    def _():
        sides[1] = jnp.zeros(sides.shape[1:], sides.dtype)

    own_copies[0].wait()
    own_copies[1].wait()
    process(tp)
    shared_hidden(tp)
    for copy in weight_copies:
        copy.wait()

    def hop(k, carry):
        for side in range(2):
            block = tp - k if side == 0 else tp + k
            inside = block >= 0 if side == 0 else block < tp_count

            @pl.when(inside)
            def _():
                for copy in send_second(side, block, False):
                    copy.wait_recv()

                @pl.when(exists(side))
                def _():
                    for copy in send_second(side, block, False):
                        copy.start()

            start_own_first(side, k)

            @pl.when(inside)
            def _():
                process(block)
                shared_hidden(block)

        experts_at(k - 1)
        return carry

    lax.fori_loop(1, tp_count, hop, 0)
    own_copies[2].wait()

    def partial_of(block):
        pieces = []
        for d in range(ep_count):
            hit, number = places_of(block, d)
            pieces.append(jnp.where(hit, metag[block, pl.ds(experts + number, 1), :], 0.0))
        weights = jnp.concatenate(pieces, axis=0)
        high = weights.astype(jnp.bfloat16)
        low = (weights - high.astype(jnp.float32)).astype(jnp.bfloat16)
        turned = (((0,), (0,)), ((), ()))

        def value(span):
            picked = back[block, :, span]
            return (
                lax.dot_general(high, picked, turned, preferred_element_type=jnp.float32)
                + lax.dot_general(low, picked, turned, preferred_element_type=jnp.float32)
                + jnp.dot(hidden[block], sdown[:, span], preferred_element_type=jnp.float32)
            )

        return value

    def wait_return(block):
        for d in range(1, ep_count):
            return_copy(block, d).wait_recv()

    def reduce_step(step):
        for side in range(2):
            block = step - tp if side == 0 else 2 * (tp_count - 1) - step - tp
            active = (block > tp) & (block < tp_count) if side == 0 else (block < tp) & (block >= 0)

            @pl.when(active)
            def _():
                wait_return(block)
                value = partial_of(block)

                def one_part(part, carry):
                    span = part_span(part)
                    own = value(span)

                    @pl.when(tp > 0 if side == 0 else tp < tp_count - 1)
                    def _():
                        pass_on(side, block, part).wait_recv()

                    psend[block, :, span] = (
                        own + sides[side, block, :, span].astype(jnp.float32)
                    ).astype(jnp.bfloat16)
                    pass_on(side, block, part).start()
                    return carry

                lax.fori_loop(0, parts, one_part, 0)

    def hop_first(k, carry):
        for side in range(2):
            block = tp - k if side == 0 else tp + k
            inside = block >= 0 if side == 0 else block < tp_count

            @pl.when(inside)
            def _():
                send_first(side, block, False).wait_recv()

                @pl.when(exists(side))
                def _():
                    send_first(side, block, False).start()

        @pl.when(k == 1)
        def _():
            experts_at(tp_count - 1)
            give_back(tp)

        reduce_step(2 * k - 1)
        reduce_step(2 * k)
        return carry

    lax.fori_loop(1, tp_count, hop_first, 0)
    wait_return(tp)
    own_value = partial_of(tp)

    def last_part(part, carry):
        span = part_span(part)
        own = own_value(span)

        @pl.when(tp > 0)
        def _():
            pass_on(0, tp, part).wait_recv()

        @pl.when(tp < tp_count - 1)
        def _():
            pass_on(1, tp, part).wait_recv()

        out[:, span] = (
            own
            + sides[0, tp, :, span].astype(jnp.float32)
            + sides[1, tp, :, span].astype(jnp.float32)
        ).astype(jnp.bfloat16)
        return carry

    lax.fori_loop(0, parts, last_part, 0)

    def finish(block, carry):
        for d in range(1, ep_count):
            return_copy(block, d).wait_send()
        for side in range(2):
            passed = block <= tp if side == 0 else block >= tp
            summed = block > tp if side == 0 else block < tp

            @pl.when(exists(side) & passed)
            def _():
                for copy in send_second(side, block, False):
                    copy.wait_send()
                send_first(side, block, False).wait_send()

            @pl.when(summed)
            def _():
                for part in range(parts):
                    pass_on(side, block, part).wait_send()

        return carry

    lax.fori_loop(0, tp_count, finish, 0)


def layer(second, first, meta, gate, up, down, sgate, sup, sdown, ep_count, tp_count, slots):
    rows, width = second.shape
    vmem = pl.BlockSpec(memory_space=pltpu.VMEM)
    hbm = pl.BlockSpec(memory_space=pl.ANY)
    dma = pltpu.SemaphoreType.DMA
    bf16 = jnp.bfloat16
    total = ep_count * slots
    return pl.pallas_call(
        functools.partial(layer_kernel, ep_count, tp_count, slots),
        out_shape=(
            jax.ShapeDtypeStruct((rows, width), bf16),
            jax.ShapeDtypeStruct((tp_count, rows, width), bf16),
        ),
        in_specs=[vmem] * 3 + [hbm] * 3 + [vmem] * 3,
        out_specs=(vmem, vmem),
        scratch_shapes=[
            pltpu.VMEM((tp_count, rows, width), bf16),
            pltpu.VMEM((tp_count,) + meta.shape, jnp.float32),
            pltpu.VMEM((tp_count, total, width), bf16),
            pltpu.VMEM((tp_count, total, width), bf16),
            pltpu.VMEM((tp_count, total, width), bf16),
            pltpu.VMEM((2, tp_count, rows, width), bf16),
            pltpu.VMEM((tp_count, rows, width), bf16),
            pltpu.VMEM(gate.shape[1:], bf16),
            pltpu.VMEM(up.shape[1:], bf16),
            pltpu.VMEM(down.shape[1:], bf16),
            pltpu.VMEM((tp_count, rows, sgate.shape[1]), bf16),
            pltpu.VMEM((total, gate.shape[2]), bf16),
            dma((3,)),
            dma((3,)),
            dma((2, tp_count)),
            dma((tp_count,)),
            dma((2, tp_count)),
            dma((tp_count,)),
            dma((2, tp_count)),
            dma((tp_count,)),
            dma((tp_count, ep_count)),
            dma((tp_count, ep_count)),
            dma((tp_count, ep_count)),
            dma((tp_count, ep_count)),
            dma((tp_count, width // CHUNK)),
            dma((2, tp_count, width // CHUNK)),
        ],
        compiler_params=pltpu.CompilerParams(
            collective_id=0, has_side_effects=True, vmem_limit_bytes=VMEM_LIMIT
        ),
        name="layer",
    )(second, first, meta, gate, up, down, sgate, sup, sdown)


def body(
    mixer_in,
    mixer_gain,
    w_query,
    w_key,
    w_value,
    sink_logit,
    moe_in,
    moe_gain,
    router,
    routes,
    expert_gate,
    expert_up,
    expert_down,
    shared_gate,
    shared_up,
    shared_down,
):
    tokens = mixer_in.shape[0]
    ep_count, tp_count = lax.axis_size("ep"), lax.axis_size("tp")
    top_count = routes.shape[1]
    experts = router.shape[1]
    capacity = 3 * top_count * tokens // (2 * experts)
    slots = -(-capacity // 16) * 16
    normed_second = rms_rows(moe_in, moe_gain)
    normed_first = rms_rows(mixer_in, mixer_gain)
    affinity = jax.nn.sigmoid(jnp.dot(normed_second, router, preferred_element_type=jnp.float32))
    hits = jnp.any(
        routes[:, :, None] == jnp.arange(experts, dtype=jnp.int32)[None, None, :], axis=1
    )
    chosen = jnp.where(hits, affinity, 0.0)
    route_weight = ROUTED_SCALE * chosen / jnp.sum(chosen, axis=-1, keepdims=True)
    earlier = jnp.tril(jnp.ones((tokens, tokens), jnp.bfloat16), -1)
    before = jnp.dot(earlier, hits.astype(jnp.bfloat16), preferred_element_type=jnp.float32)
    places = jnp.where(hits, before, -1.0)
    meta = jnp.concatenate([places, route_weight], axis=1).T
    width = normed_second.shape[1]
    moe_out, gathered_first = layer(
        normed_second, normed_first, meta, expert_gate, expert_up, expert_down,
        shared_gate, shared_up, shared_down, ep_count, tp_count, slots,
    )
    query_cols = w_query.shape[1]
    key_cols = w_key.shape[1]
    joined = jnp.concatenate([w_query, w_key, w_value], axis=1)
    projected = jnp.dot(
        gathered_first.reshape(-1, width), joined, preferred_element_type=jnp.float32
    )
    span_rows = projected.shape[0]
    offset = lax.axis_index("ep") * span_rows
    seq_length = span_rows * ep_count
    positions = offset + jnp.arange(span_rows, dtype=jnp.int32)
    query_rows = rotate(
        projected[:, :query_cols].reshape(span_rows, -1, HEAD_DIM), positions
    ).astype(jnp.bfloat16)
    key_rows = rotate(
        projected[:, query_cols : query_cols + key_cols].reshape(span_rows, -1, HEAD_DIM), positions
    ).astype(jnp.bfloat16)
    value_rows = projected[:, query_cols + key_cols :].astype(jnp.bfloat16)
    stacked = jnp.concatenate([key_rows.reshape(span_rows, key_cols), value_rows], axis=1)
    padded = extended(stacked, (("ep", 0),), WINDOW)
    mixed = attend(query_rows, padded, sink_logit, offset, seq_length)
    return (mixed, moe_out)


def solution(mesh):
    return jax.shard_map(
        body,
        mesh=mesh,
        in_specs=(
            P(("grp", "ep", "tp"), None),
            P(),
            P(None, "tp"),
            P(None, "tp"),
            P(None, "tp"),
            P("tp"),
            P(("grp", "ep", "tp"), None),
            P(),
            P(),
            P(("grp", "ep", "tp"), None),
            P(("ep", "tp"), None, None),
            P(("ep", "tp"), None, None),
            P(("ep", "tp"), None, None),
            P(None, "tp"),
            P(None, "tp"),
            P("tp", None),
        ),
        out_specs=(P(("grp", "ep"), "tp"), P(("grp", "ep", "tp"), None)),
        check_vma=False,
    )
```

profile of v0, /device:TPU:1, one launch (start us, length us, event | category | flops | bytes accessed | tf_op | source)
XLA Modules:
  0.0 139.3 jit_solution(12043619239715672302)
XLA Ops:
  0.6 0.0 copy-start
  0.7 1.3 fusion.16
  1.9 1.2 fusion.19
  3.2 0.7 fusion.29
  3.9 0.2 convolution_select_fusion
  4.1 2.2 %fusion.18 = (bf16[128,2048]{1,0:T(8,128)(2,1)S(1)}, bf16[128,2048]{1,0:T(8,128)(2,1)}) fusion(bf16[128,2048]{1,0:T(8,128)(2,1)} %param.22, f32[2048]{0:T(1024)} %param.23, f32[128]{0:T(128)S(1)} %add_rsqrt_fusion.1, f32[2048]{0:T(1024)} %param.17, f32[128]{0:T(128)S(1)} %add_rsqrt_fusion, bf16[128,2048]{1,0:T(8,128)(2,1)} %param.16), kind=kLoop, calls=%fused_computation.28 | loop fusion | flops 2097152 | bytes 2114560 | tf_op jit(solution)/shard_map/convert_element_type | solution.py:35
  6.3 0.0 copy-start.1
  6.3 0.0 copy-done
  6.3 0.3 fusion.42
  6.6 0.6 maximum_bitcast_fusion.meta
  7.2 0.0 copy-done.1
  7.2 114.6 %layer.1 = (bf16[128,2048]{1,0:T(8,128)(2,1)}, bf16[4,128,2048]{2,1,0:T(8,128)(2,1)}) custom-call(bf16[128,2048]{1,0:T(8,128)(2,1)} %copy-done.1, bf16[128,2048]{1,0:T(8,128)(2,1)} %get-tuple-element.52.first, f32[32,128]{1,0:T(8,128)} %maximum_bitcast_fusion.meta, bf16[1,2048,512]{2,1,0:T(8,128)(2,1)} %gate_hbm.1, bf16[1,2048,512]{2,1,0:T(8,128)(2,1)} %up_hbm.1, ...), custom_call_target="tpu_custom_call" | custom-call | tf_op jit(solution)/shard_map/layer/pallas_call | solution.py:449
  121.9 3.5 %fusion.3 = f32[512,512]{0,1:T(8,128)S(1)} fusion(bf16[512,2048]{1,0:T(8,128)(2,1)} %bitcast.47, bf16[2048,128]{1,0:T(8,128)(2,1)} %param.20, bf16[2048,128]{1,0:T(8,128)(2,1)} %param.19, bf16[2048,256]{1,0:T(8,128)(2,1)} %param.18), kind=kOutput, calls=%fused_computation.6 | convolution fusion | flops 1080033280 | bytes 5242880 | tf_op jit(solution)/shard_map/dot_general | solution.py:536
  125.3 0.0 copy-start.3
  125.4 0.3 multiply_cosine_fusion
  125.8 2.9 %collective-permute-start.1 = (bf16[128,256]{0,1:T(8,128)(2,1)S(1)}, bf16[128,256]{0,1:T(8,128)(2,1)S(1)}, u32[]{:S(2)}, u32[]{:S(2)}) collective-permute-start(bf16[128,256]{0,1:T(8,128)(2,1)S(1)} %get-tuple-element.44), channel_id=1, source_target_pairs={{4,0},{8,4},{12,8},{5,1},{9,5},{13,9},{6,2},{10,6},{14,10},{7,3},{... | collective-permute-start | bytes 196616 | tf_op jit(solution)/shard_map/ppermute | solution.py:27
  128.7 2.9 %collective-permute-start = (bf16[128,256]{0,1:T(8,128)(2,1)S(1)}, bf16[128,256]{0,1:T(8,128)(2,1)S(1)}, u32[]{:S(2)}, u32[]{:S(2)}) collective-permute-start(bf16[128,256]{0,1:T(8,128)(2,1)S(1)} %get-tuple-element.43), channel_id=1, source_target_pairs={{0,4},{4,8},{8,12},{1,5},{5,9},{9,13},{2,6},{6,10},{10,14},{3,7},{... | collective-permute-start | bytes 196616 | tf_op jit(solution)/shard_map/ppermute | solution.py:24
  131.7 0.1 subtract_convert_fusion
  131.7 0.8 fusion.10
  132.5 0.0 copy-done.3
  132.5 0.1 max.22
  132.6 0.0 collective-permute-done.1
  132.6 0.1 collective-permute-done
  132.8 1.3 fusion.1
  134.1 0.1 broadcast_maximum_fusion
  134.1 1.4 fusion
  135.5 0.1 exponential_add_fusion
  135.6 0.0 copy-start.2
  135.6 2.0 %fusion.11 = bf16[2,64,2,512]{3,1,2,0:T(8,128)(2,1)S(1)} fusion(bf16[768,2,64,1]{0,2,3,1:T(8,128)(2,1)S(1)} %bitcast.43, f32[2,768,512,2]{2,1,3,0:T(8,128)S(1)} %get-tuple-element.50, f32[2,2,512]{2,1,0:T(2,128)S(1)} %exponential_add_fusion, f32[2,2,512]{2,1,0:T(2,128)S(1)} %broadcast_maximum_fusion, pred[512,768]{0,1:T(8,128)(4,1)S(1)} %fusion.10), kind=kOutput, calls=%fused_computation.19 | convolution fusion | flops 209321984 | bytes 7159808 | tf_op jit(solution)/shard_map/while/body/eval_jaxpr/kgqc,ckd->qkgd/dot_general | solution.py:85
  137.6 0.8 copy.22
  138.5 0.0 copy-done.2
  138.5 0.8 copy.27
  (16 shorter events, 0.3 us)
Async XLA Ops:
  0.6 5.7 %copy-start = (bf16[2048,16]{0,1:T(8,128)(2,1)S(1)}, bf16[2048,16]{0,1:T(8,128)(2,1)}, u32[]{:S(2)}) copy-start(bf16[2048,16]{0,1:T(8,128)(2,1)} %param.24) | copy-start | bytes 196612
  6.3 0.9 copy-start.1
  125.3 7.2 %copy-start.3 = (f32[4]{0:T(128)S(1)}, f32[4]{0:T(128)}, u32[]{:S(2)}) copy-start(f32[4]{0:T(128)} %param.21) | copy-start | bytes 52
  125.8 6.8 %collective-permute-start.1 = (bf16[128,256]{0,1:T(8,128)(2,1)S(1)}, bf16[128,256]{0,1:T(8,128)(2,1)S(1)}, u32[]{:S(2)}, u32[]{:S(2)}) collective-permute-start(bf16[128,256]{0,1:T(8,128)(2,1)S(1)} %get-tuple-element.44), channel_id=1, source_target_pairs={{4,0},{8,4},{12,8},{5,1},{9,5},{13,9},{6,2},{10,6},{14,10},{7,3},{... | collective-permute-start | bytes 196616 | tf_op jit(solution)/shard_map/ppermute | solution.py:27
  128.7 4.0 %collective-permute-start = (bf16[128,256]{0,1:T(8,128)(2,1)S(1)}, bf16[128,256]{0,1:T(8,128)(2,1)S(1)}, u32[]{:S(2)}, u32[]{:S(2)}) collective-permute-start(bf16[128,256]{0,1:T(8,128)(2,1)S(1)} %get-tuple-element.43), channel_id=1, source_target_pairs={{0,4},{4,8},{8,12},{1,5},{5,9},{9,13},{2,6},{6,10},{10,14},{3,7},{... | collective-permute-start | bytes 196616 | tf_op jit(solution)/shard_map/ppermute | solution.py:24
  135.6 2.9 %copy-start.2 = (bf16[128,2048]{1,0:T(8,128)(2,1)S(1)}, bf16[128,2048]{1,0:T(8,128)(2,1)}, u32[]{:S(2)}) copy-start(bf16[128,2048]{1,0:T(8,128)(2,1)} %get-tuple-element.60) | copy-start | bytes 1572868
where the time goes:
time: 140 us; the launch traced here: 139 us
  Pallas kernels  115 us (82%)
  other arithmetic  8.89 us (6%)
  matrix products  7.21 us (5%)
  starting transfers between devices  5.74 us (4%)
  local copies, waits for them, and re-layouts  1.85 us (1%)
    pallas_call x1, Pallas kernels, layer(): pl.pallas_call(functools.partial(layer_kernel, ep_count, tp_count, slots)...  115 us
    dot_general x1, matrix products, body(): jnp.dot(gathered_first.reshape(-1, width), joined, preferred_element_type...  3.47 us
    ppermute x1, starting transfers between devices, extended(): lax.ppermute(lax.slice_in_dim(block, block.shape[dim] - width, None, axis...  2.89 us
    ppermute x1, starting transfers between devices, extended(): lax.ppermute(lax.slice_in_dim(block, 0, width, axis=dim), axis, backward)  2.85 us
  transfers between devices with their start and end apart: 2, of which 1 were waited for; matrix products, arithmetic and copies ran while one was open for 1% of the time, Pallas kernels for 0%

commit v1 on v0

v1 whole, which is shorter than its diff:
```python
import functools

import jax
import jax.numpy as jnp
from jax import lax
from jax.experimental import pallas as pl
from jax.experimental.pallas import tpu as pltpu
from jax.sharding import PartitionSpec as P

HEAD_DIM = 64
WINDOW = 128
EPS = 1e-06
THETA = 10000.0
ROUTED_SCALE = 2.5
LANES = 128
CHUNK = 512
MESH = pl.DeviceIdType.MESH
VMEM_LIMIT = 63 * 2**20


def remote(src, dst, send_sem, recv_sem, device):
    return pltpu.make_async_remote_copy(
        src_ref=src,
        dst_ref=dst,
        send_sem=send_sem,
        recv_sem=recv_sem,
        device_id=device,
        device_id_type=MESH,
    )


def greet(grp, ep, tp, ep_count, tp_count):
    barrier = pltpu.get_barrier_semaphore()

    @pl.when(tp > 0)
    def _():
        pl.semaphore_signal(barrier, inc=1, device_id=(grp, ep, tp - 1), device_id_type=MESH)

    @pl.when(tp < tp_count - 1)
    def _():
        pl.semaphore_signal(barrier, inc=1, device_id=(grp, ep, tp + 1), device_id_type=MESH)

    for d in range(1, ep_count):
        pl.semaphore_signal(
            barrier, inc=1, device_id=(grp, lax.rem(ep + d, ep_count), tp), device_id_type=MESH
        )
    return barrier


def layer_kernel(
    ep_count, tp_count, slots,
    second_in, gain_second, gain_first, router, routes, inverse, sink,
    first_hbm, gate_hbm, up_hbm, down_hbm, sgate_hbm, sup_hbm, sdown_hbm, wq_hbm, wk_hbm, wv_hbm,
    out, mixed,
    gath2, gath1, first_in, metag, sbuf, disp, back, sides, psend,
    gate, up, down, sgate, sup, sdown, wq, wk, wv,
    hidden, hexp, cosine, sine, qbuf, kvbuf,
    l_sem, s2, r2, sm, rm, s1, r1, sd, rd, sb, rb, sp, rs, hs, hr,
):
    grp, ep, tp = lax.axis_index("grp"), lax.axis_index("ep"), lax.axis_index("tp")
    rows, width = second_in.shape
    experts = metag.shape[1] // 2
    total = ep_count * slots
    parts = width // CHUNK
    f32, bf16 = jnp.float32, jnp.bfloat16
    away = pl.ds(slots, total - slots)

    local = [
        pltpu.make_async_copy(src, dst, l_sem.at[i])
        for i, (src, dst) in enumerate(
            [
                (first_hbm, first_in),
                (sgate_hbm, sgate),
                (sup_hbm, sup),
                (gate_hbm.at[0], gate),
                (up_hbm.at[0], up),
                (down_hbm.at[0], down),
                (wq_hbm, wq),
                (wk_hbm, wk),
                (wv_hbm, wv),
                (sdown_hbm, sdown),
            ]
        )
    ]
    for copy in local:
        copy.start()
    barrier = greet(grp, ep, tp, ep_count, tp_count)

    def toward(side):
        return (grp, ep, tp + (1 if side == 0 else -1))

    def exists(side):
        return tp < tp_count - 1 if side == 0 else tp > 0

    def peer(d):
        return (grp, lax.rem(ep + d, ep_count), tp)

    def part_span(part, size=CHUNK):
        return pl.ds(pl.multiple_of(part * size, size), size)

    def each_part(body, count=parts):
        def step(part, carry):
            body(part)
            return carry

        lax.fori_loop(0, count, step, 0)

    def at(side, distance):
        block = tp - distance if side == 0 else tp + distance
        return block, (block >= 0 if side == 0 else block < tp_count)

    def send_second(side, block, part):
        ref = gath2.at[block, :, part_span(part)]
        return remote(ref, ref, s2.at[side, block], r2.at[block, part], toward(side))

    def send_meta(side, block):
        return remote(metag.at[block], metag.at[block], sm.at[side, block], rm.at[block], toward(side))

    def send_first(side, block):
        return remote(gath1.at[block], gath1.at[block], s1.at[side, block], r1.at[block], toward(side))

    def dispatch_copy(block, d, span):
        mine = pl.ds(d * slots, slots)
        return remote(sbuf.at[block, mine, span], disp.at[block, mine, span], sd.at[block], rd.at[block], peer(d))

    def dispatch_all(block):
        return remote(sbuf.at[block, away], disp.at[block, away], sd.at[block], rd.at[block], peer(1))

    def return_copy(block, d, part):
        mine, span = pl.ds(d * slots, slots), part_span(part)
        return remote(
            sbuf.at[block, mine, span], back.at[block, mine, span],
            sb.at[block], rb.at[block, part], peer(ep_count - d),
        )

    def return_part(block, part):
        span = part_span(part)
        return remote(
            sbuf.at[block, away, span], back.at[block, away, span], sb.at[block], rb.at[block, part], peer(1)
        )

    def return_all(block):
        return remote(sbuf.at[block, away], back.at[block, away], sb.at[block], rb.at[block, 0], peer(1))

    def pass_on(side, block, part):
        span = part_span(part)
        return remote(
            psend.at[block, :, span], sides.at[side, block, :, span],
            sp.at[block, part], rs.at[side, block, part], toward(side),
        )

    def halo(side):
        source = tp_count * rows if side == 0 else rows
        target = 0 if side == 0 else (tp_count + 1) * rows
        return remote(
            kvbuf.at[pl.ds(source, rows)], kvbuf.at[pl.ds(target, rows)],
            hs.at[side], hr.at[side], (grp, ep + (1 if side == 0 else -1), tp),
        )

    def normalize(source, gain, target):
        def squares(part, carry):
            values = source[:, part_span(part)].astype(f32)
            return carry + jnp.sum(values * values, axis=1, keepdims=True)

        summed = lax.fori_loop(0, parts, squares, jnp.zeros((rows, 1), f32))
        factor = lax.rsqrt(summed / width + EPS)

        def scale(part):
            span = part_span(part)
            target[:, span] = (source[:, span].astype(f32) * factor * gain[:, span]).astype(bf16)

        each_part(scale)

    def places_of(block, d):
        expert = lax.rem(ep + d, ep_count) * tp_count + tp
        slot_ids = lax.broadcasted_iota(jnp.int32, (slots, rows), 0).astype(f32)
        return slot_ids == metag[block, pl.ds(expert, 1), :], expert

    def pick_part(block, part):
        span = part_span(part)
        picks = [jnp.where(places_of(block, d)[0], 1.0, 0.0) for d in range(ep_count)]
        pick = jnp.concatenate(picks, axis=0).astype(bf16)
        picked = jnp.dot(pick, gath2[block, :, span], preferred_element_type=f32).astype(bf16)
        disp[block, 0:slots, span] = picked[0:slots]
        sbuf[block, slots:total, span] = picked[slots:total]
        for d in range(1, ep_count):
            dispatch_copy(block, d, span).start()

    def shared_hidden(block):
        values = gath2[block]
        gated = jnp.dot(values, sgate[...], preferred_element_type=f32)
        lifted = jnp.dot(values, sup[...], preferred_element_type=f32)
        hidden[block] = (jax.nn.silu(gated) * lifted).astype(bf16)

    def expert(block):
        dispatch_all(block).wait()

        def units(part):
            span = part_span(part, 256)
            values = disp[block]
            gated = jnp.dot(values, gate[:, span], preferred_element_type=f32)
            lifted = jnp.dot(values, up[:, span], preferred_element_type=f32)
            hexp[:, span] = (jax.nn.silu(gated) * lifted).astype(bf16)

        each_part(units, gate.shape[1] // 256)

        def columns(part):
            span = part_span(part)
            result = jnp.dot(hexp[...], down[:, span], preferred_element_type=f32).astype(bf16)
            back[block, 0:slots, span] = result[0:slots]
            sbuf[block, slots:total, span] = result[slots:total]

            @pl.when(block != tp)
            def _():
                for d in range(1, ep_count):
                    return_copy(block, d, part).start()

        each_part(columns)

    def experts_at(distance):
        def one(side, carry):
            block = tp + (2 * side - 1) * distance

            @pl.when((block >= 0) & (block < tp_count) & ((distance > 0) | (side == 0)))
            def _():
                expert(block)

            return carry

        lax.fori_loop(0, 2, one, 0)

    def start_own_first(side, step):
        last = tp if side == 0 else tp_count - 1 - tp

        @pl.when(exists(side) & (step == last))
        def _():
            send_first(side, tp).start()

    def rotated(values, cos_rows, sin_rows):
        pieces = []
        half = HEAD_DIM // 2
        size = LANES if values.shape[1] % LANES == 0 else HEAD_DIM
        for start in range(0, values.shape[1], size):
            piece = values[:, start : start + size]
            if size == LANES:
                lane = lax.broadcasted_iota(jnp.int32, piece.shape, 1)
                swapped = jnp.where(
                    lax.rem(lane, HEAD_DIM) < half,
                    pltpu.roll(piece, LANES - half, 1),
                    pltpu.roll(piece, half, 1),
                )
            else:
                swapped = jnp.concatenate([piece[:, half:], piece[:, :half]], axis=1)
            pieces.append(piece * cos_rows[:, :size] + swapped * sin_rows[:, :size])
        return pieces[0] if len(pieces) == 1 else jnp.concatenate(pieces, axis=1)

    def project(block):
        base = pl.multiple_of(block * rows, rows)
        values = gath1[block]
        cos_rows, sin_rows = cosine[pl.ds(base, rows), :], sine[pl.ds(base, rows), :]
        query = jnp.dot(values, wq[...], preferred_element_type=f32)
        key = jnp.dot(values, wk[...], preferred_element_type=f32)
        value = jnp.dot(values, wv[...], preferred_element_type=f32)
        qbuf[pl.ds(base, rows), :] = rotated(query, cos_rows, sin_rows).astype(bf16)
        kvbuf[pl.ds(pl.multiple_of(base + rows, rows), rows), :] = jnp.concatenate(
            [rotated(key, cos_rows, sin_rows), value], axis=1
        ).astype(bf16)

    def tables():
        def one(block):
            start = pl.multiple_of(block * rows, rows)
            shape = (rows, LANES)
            place = ep * (tp_count * rows) + start + lax.broadcasted_iota(jnp.int32, shape, 0)
            angle = place.astype(f32) * inverse[...]
            lane = lax.broadcasted_iota(jnp.int32, shape, 1)
            turn = jnp.sin(angle)
            cosine[pl.ds(start, rows), :] = jnp.cos(angle)
            sine[pl.ds(start, rows), :] = jnp.where(lax.rem(lane, HEAD_DIM) < HEAD_DIM // 2, -turn, turn)

        each_part(one, tp_count)

    kv_heads = wk.shape[1] // HEAD_DIM
    group = wq.shape[1] // wk.shape[1]

    def attend(block):
        base = pl.multiple_of(block * rows, rows)
        window = kvbuf[pl.ds(base, 3 * rows), :]
        query = qbuf[pl.ds(base, rows), :]
        shape = (rows, 3 * rows)
        row = lax.broadcasted_iota(jnp.int32, shape, 0)
        col = lax.broadcasted_iota(jnp.int32, shape, 1)
        gap = col - row - rows
        low = jnp.where((ep == 0) & (block == 0), rows, 0)
        high = jnp.where((ep == ep_count - 1) & (block == tp_count - 1), 2 * rows, 3 * rows)
        near = (gap <= WINDOW) & (gap >= -WINDOW) & (col >= low) & (col < high)
        pieces = []
        for g in range(kv_heads):
            keys = window[:, g * HEAD_DIM : (g + 1) * HEAD_DIM]
            start = (kv_heads + g) * HEAD_DIM
            values = window[:, start : start + HEAD_DIM]
            for h in range(g * group, (g + 1) * group):
                scores = lax.dot_general(
                    query[:, h * HEAD_DIM : (h + 1) * HEAD_DIM], keys, (((1,), (1,)), ((), ())),
                    preferred_element_type=f32,
                ) * HEAD_DIM ** (-0.5)
                scores = jnp.where(near, scores, -jnp.inf)
                bound = sink[0, h]
                top = jnp.maximum(jnp.max(scores, axis=1, keepdims=True), bound)
                weights = jnp.exp(scores - top)
                summed = jnp.sum(weights, axis=1, keepdims=True) + jnp.exp(bound - top)
                share = (weights * (1.0 / summed)).astype(bf16)
                pieces.append(jnp.dot(share, values, preferred_element_type=f32))
        mixed[pl.ds(base, rows), :] = jnp.concatenate(pieces, axis=1).astype(bf16)

    normalize(second_in, gain_second, gath2.at[tp])
    ids = lax.broadcasted_iota(jnp.int32, (experts, rows), 0)
    hit = ids == routes[0:1, :]
    for j in range(1, routes.shape[0]):
        hit = hit | (ids == routes[j : j + 1, :])
    earlier = (
        lax.broadcasted_iota(jnp.int32, (rows, rows), 0) < lax.broadcasted_iota(jnp.int32, (rows, rows), 1)
    )
    before = jnp.dot(
        jnp.where(hit, 1.0, 0.0).astype(bf16), jnp.where(earlier, 1.0, 0.0).astype(bf16),
        preferred_element_type=f32,
    )
    metag[tp, 0:experts, :] = jnp.where(hit, before, -1.0)
    pl.semaphore_wait(barrier, ep_count + jnp.where((tp > 0) & (tp < tp_count - 1), 1, 0))
    def send_own(part):
        for side in range(2):

            @pl.when(exists(side))
            def _():
                send_second(side, tp, part).start()

    send_own(0)
    affinity = lax.dot_general(
        router[...], gath2[tp], (((1,), (1,)), ((), ())), preferred_element_type=f32
    )
    chosen = jnp.where(hit, jax.nn.sigmoid(affinity), 0.0)
    metag[tp, experts : 2 * experts, :] = ROUTED_SCALE * chosen / jnp.sum(chosen, axis=0, keepdims=True)
    pick_part(tp, 0)
    for side in range(2):

        @pl.when(exists(side))
        def _():
            send_meta(side, tp).start()

    for part in range(1, parts):
        send_own(part)

    def pick_rest(part, carry):
        pick_part(tp, part)
        return carry

    lax.fori_loop(1, parts, pick_rest, 0)
    local[0].wait()
    normalize(first_in, gain_first, gath1.at[tp])
    for side in range(2):
        start_own_first(side, 0)

    @pl.when(tp == 0)
    def _():
        sides[0] = jnp.zeros(sides.shape[1:], sides.dtype)

    @pl.when(tp == tp_count - 1)
    def _():
        sides[1] = jnp.zeros(sides.shape[1:], sides.dtype)

    @pl.when(ep == 0)
    def _():
        kvbuf[0:rows, :] = jnp.zeros((rows, kvbuf.shape[1]), bf16)

    @pl.when(ep == ep_count - 1)
    def _():
        kvbuf[(tp_count + 1) * rows : (tp_count + 2) * rows, :] = jnp.zeros((rows, kvbuf.shape[1]), bf16)

    for copy in local[1:]:
        copy.wait()
    shared_hidden(tp)

    def weights_of(block):
        pieces = []
        for d in range(ep_count):
            hit_rows, number = places_of(block, d)
            pieces.append(jnp.where(hit_rows, metag[block, pl.ds(experts + number, 1), :], 0.0))
        weights = jnp.concatenate(pieces, axis=0)
        top = weights.astype(bf16)
        return top, (weights - top.astype(f32)).astype(bf16)

    def value_of(block, weights, span):
        turned = (((0,), (0,)), ((), ()))
        picked = back[block, :, span]
        return (
            lax.dot_general(weights[0], picked, turned, preferred_element_type=f32)
            + lax.dot_general(weights[1], picked, turned, preferred_element_type=f32)
            + jnp.dot(hidden[block], sdown[:, span], preferred_element_type=f32)
        )

    def reduce_step(step):
        for side in range(2):
            block = step - tp if side == 0 else 2 * (tp_count - 1) - step - tp
            active = (block > tp) & (block < tp_count) if side == 0 else (block < tp) & (block >= 0)

            @pl.when(active)
            def _():
                weights = weights_of(block)

                def one_part(part):
                    span = part_span(part)
                    return_part(block, part).wait_recv()
                    own = value_of(block, weights, span)

                    @pl.when(tp > 0 if side == 0 else tp < tp_count - 1)
                    def _():
                        pass_on(side, block, part).wait_recv()

                    psend[block, :, span] = (own + sides[side, block, :, span].astype(f32)).astype(bf16)
                    pass_on(side, block, part).start()

                each_part(one_part)

    early = tp_count > 2

    def hop(k, carry):
        def one_part(part):
            for side in range(2):
                block, inside = at(side, k)

                @pl.when(inside)
                def _():
                    send_second(side, block, part).wait_recv()

                    @pl.when(exists(side))
                    def _():
                        send_second(side, block, part).start()

                    @pl.when(part == 0)
                    def _():
                        send_meta(side, block).wait_recv()

                        @pl.when(exists(side))
                        def _():
                            send_meta(side, block).start()

            for side in range(2):
                block, inside = at(side, k)

                @pl.when(inside)
                def _():
                    pick_part(block, part)

        each_part(one_part)
        for side in range(2):
            start_own_first(side, k)
        for side in range(2):
            block, inside = at(side, k)

            @pl.when(inside)
            def _():
                shared_hidden(block)

        if early:

            @pl.when(k == tp_count - 1)
            def _():
                reduce_step(1)

        experts_at(k - 1)

        @pl.when(k == 1)
        def _():
            tables()
            project(tp)

        return carry

    lax.fori_loop(1, tp_count, hop, 0)
    experts_at(tp_count - 1)
    for part in range(parts):
        for d in range(1, ep_count):
            return_copy(tp, d, part).start()

    def start_halo(block):
        @pl.when((block == tp_count - 1) & (ep < ep_count - 1))
        def _():
            halo(0).start()

        @pl.when((block == 0) & (ep > 0))
        def _():
            halo(1).start()

    start_halo(tp)

    def attend_inner(block):
        @pl.when((block > 0) & (block < tp_count - 1))
        def _():
            attend(block)

    def first_hop(k, carry):
        for side in range(2):
            block, inside = at(side, k)

            @pl.when(inside & exists(side))
            def _():
                send_first(side, block).wait_recv()
                send_first(side, block).start()

        reduce_step(jnp.where(k == 1, 2 if early else 1, 2 * k - 1))
        for side in range(2):
            block, inside = at(side, k)

            @pl.when(inside & jnp.logical_not(exists(side)))
            def _():
                send_first(side, block).wait_recv()

        def use(side, carry):
            block = tp + (2 * side - 1) * k

            @pl.when((block >= 0) & (block < tp_count))
            def _():
                project(block)
                start_halo(block)

            return carry

        lax.fori_loop(0, 2, use, 0)

        def settle(side, carry):
            block = tp + (2 * side - 1) * (k - 1)

            @pl.when((block > 0) & (block < tp_count - 1) & ((k > 1) | (side == 0)))
            def _():
                attend(block)

            return carry

        lax.fori_loop(0, 2, settle, 0)

        @pl.when(k == jnp.maximum(tp, tp_count - 1 - tp))
        def _():
            @pl.when(ep < ep_count - 1)
            def _():
                halo(1).wait_recv()

            @pl.when(ep > 0)
            def _():
                halo(0).wait_recv()

            def edge(side, carry):
                attend((tp_count - 1) * (1 - side))
                return carry

            lax.fori_loop(0, 2, edge, 0)

        if early:

            @pl.when(k > 1)
            def _():
                reduce_step(2 * k)

        return carry

    lax.fori_loop(1, tp_count, first_hop, 0)
    own_weights = weights_of(tp)

    def last_part(part):
        span = part_span(part)
        return_part(tp, part).wait_recv()
        own = value_of(tp, own_weights, span)

        @pl.when(tp > 0)
        def _():
            pass_on(0, tp, part).wait_recv()

        @pl.when(tp < tp_count - 1)
        def _():
            pass_on(1, tp, part).wait_recv()

        out[:, span] = (
            own + sides[0, tp, :, span].astype(f32) + sides[1, tp, :, span].astype(f32)
        ).astype(bf16)

    each_part(last_part)

    def finish(block):
        return_all(block).wait_send()
        for side in range(2):
            passed = block <= tp if side == 0 else block >= tp
            summed = block > tp if side == 0 else block < tp

            @pl.when(exists(side) & passed)
            def _():
                ref = gath2.at[block]
                remote(ref, ref, s2.at[side, block], r2.at[block, 0], toward(side)).wait_send()
                send_meta(side, block).wait_send()
                send_first(side, block).wait_send()

            @pl.when(summed)
            def _():
                for part in range(parts):
                    pass_on(side, block, part).wait_send()

    each_part(finish, tp_count)

    @pl.when(ep < ep_count - 1)
    def _():
        halo(0).wait_send()

    @pl.when(ep > 0)
    def _():
        halo(1).wait_send()


def layer(
    second, first, gain_second, gain_first, router, routes, inverse, sink,
    gate, up, down, sgate, sup, sdown, wq, wk, wv, ep_count, tp_count, slots,
):
    rows, width = second.shape
    experts = router.shape[0]
    vmem = pl.BlockSpec(memory_space=pltpu.VMEM)
    smem = pl.BlockSpec(memory_space=pltpu.SMEM)
    hbm = pl.BlockSpec(memory_space=pl.ANY)
    dma = pltpu.SemaphoreType.DMA
    bf16, f32 = jnp.bfloat16, jnp.float32
    total = ep_count * slots
    parts = width // CHUNK
    span = tp_count * rows
    kv_cols = wk.shape[1] + wv.shape[1]
    return pl.pallas_call(
        functools.partial(layer_kernel, ep_count, tp_count, slots),
        out_shape=(
            jax.ShapeDtypeStruct((rows, width), bf16),
            jax.ShapeDtypeStruct((span, wq.shape[1]), bf16),
        ),
        in_specs=[vmem] * 6 + [smem] + [hbm] * 10,
        out_specs=(vmem, vmem),
        scratch_shapes=[
            pltpu.VMEM((tp_count, rows, width), bf16),
            pltpu.VMEM((tp_count, rows, width), bf16),
            pltpu.VMEM((rows, width), bf16),
            pltpu.VMEM((tp_count, 2 * experts, rows), f32),
            pltpu.VMEM((tp_count, total, width), bf16),
            pltpu.VMEM((tp_count, total, width), bf16),
            pltpu.VMEM((tp_count, total, width), bf16),
            pltpu.VMEM((2, tp_count, rows, width), bf16),
            pltpu.VMEM((tp_count, rows, width), bf16),
            pltpu.VMEM(gate.shape[1:], bf16),
            pltpu.VMEM(up.shape[1:], bf16),
            pltpu.VMEM(down.shape[1:], bf16),
            pltpu.VMEM(sgate.shape, bf16),
            pltpu.VMEM(sup.shape, bf16),
            pltpu.VMEM(sdown.shape, bf16),
            pltpu.VMEM(wq.shape, bf16),
            pltpu.VMEM(wk.shape, bf16),
            pltpu.VMEM(wv.shape, bf16),
            pltpu.VMEM((tp_count, rows, sgate.shape[1]), bf16),
            pltpu.VMEM((total, gate.shape[2]), bf16),
            pltpu.VMEM((span, LANES), f32),
            pltpu.VMEM((span, LANES), f32),
            pltpu.VMEM((span, wq.shape[1]), bf16),
            pltpu.VMEM((span + 2 * rows, kv_cols), bf16),
            dma((10,)),
            dma((2, tp_count)),
            dma((tp_count, parts)),
            dma((2, tp_count)),
            dma((tp_count,)),
            dma((2, tp_count)),
            dma((tp_count,)),
            dma((tp_count,)),
            dma((tp_count,)),
            dma((tp_count,)),
            dma((tp_count, parts)),
            dma((tp_count, parts)),
            dma((2, tp_count, parts)),
            dma((2,)),
            dma((2,)),
        ],
        compiler_params=pltpu.CompilerParams(
            collective_id=0, has_side_effects=True, vmem_limit_bytes=VMEM_LIMIT
        ),
        name="layer",
    )(
        second, gain_second, gain_first, router, routes, inverse, sink,
        first, gate, up, down, sgate, sup, sdown, wq, wk, wv,
    )


def body(
    mixer_in,
    mixer_gain,
    w_query,
    w_key,
    w_value,
    sink_logit,
    moe_in,
    moe_gain,
    router,
    routes,
    expert_gate,
    expert_up,
    expert_down,
    shared_gate,
    shared_up,
    shared_down,
):
    tokens = mixer_in.shape[0]
    ep_count, tp_count = lax.axis_size("ep"), lax.axis_size("tp")
    top_count = routes.shape[1]
    experts = router.shape[1]
    capacity = 3 * top_count * tokens // (2 * experts)
    slots = -(-capacity // 16) * 16
    half = HEAD_DIM // 2
    inverse = THETA ** (-(jnp.arange(half, dtype=jnp.float32) * 2.0) / HEAD_DIM)
    moe_out, mixed = layer(
        moe_in, mixer_in, moe_gain[None, :], mixer_gain[None, :], router.T, routes.T,
        jnp.tile(inverse, LANES // half)[None, :], sink_logit[None, :],
        expert_gate, expert_up, expert_down, shared_gate, shared_up, shared_down,
        w_query, w_key, w_value, ep_count, tp_count, slots,
    )
    return (mixed, moe_out)


def solution(mesh):
    return jax.shard_map(
        body,
        mesh=mesh,
        in_specs=(
            P(("grp", "ep", "tp"), None),
            P(),
            P(None, "tp"),
            P(None, "tp"),
            P(None, "tp"),
            P("tp"),
            P(("grp", "ep", "tp"), None),
            P(),
            P(),
            P(("grp", "ep", "tp"), None),
            P(("ep", "tp"), None, None),
            P(("ep", "tp"), None, None),
            P(("ep", "tp"), None, None),
            P(None, "tp"),
            P(None, "tp"),
            P("tp", None),
        ),
        out_specs=(P(("grp", "ep"), "tp"), P(("grp", "ep", "tp"), None)),
        check_vma=False,
    )
```

time: 140 us -> 101 us (0.72)
  Pallas kernels: 115 us -> 95.7 us
  other arithmetic: 8.89 us -> 0.01 us
  matrix products: 7.21 us -> 0 us
  starting transfers between devices: 5.74 us -> 0 us
  local copies, waits for them, and re-layouts: 1.85 us -> 4.15 us
    pallas_call x1, Pallas kernels: 115 us -> 95.7 us  [layer(): pl.pallas_call(functools.partial(layer_kernel, ep_count, tp_count, slots)...]
    dot_general x5 -> x0, matrix products: 7.21 us -> none  [the longest x1 3.47 us: body(): jnp.dot(gathered_first.reshape(-1, width), joined, preferred_element_type...]
    ppermute x2 -> x0, starting transfers between devices: 5.74 us -> none  [the longest x1 2.89 us: extended(): lax.ppermute(lax.slice_in_dim(block, block.shape[dim] - width, None, axis...]
    reduce_sum x3 -> x0, other arithmetic: 3.86 us -> none  [the longest x2 2.49 us: rms_rows(): factor = lax.rsqrt(jnp.mean(values * values, axis=-1, keepdims=True) + EPS)]
    convert_element_type x1 -> x0, other arithmetic: 2.24 us -> none  [rms_rows(): return (values * factor * gain_vector).astype(jnp.bfloat16)]
    unnamed x10 -> x2, local copies, waits for them, and re-layouts: 1.66 us -> 3.55 us
  transfers between devices with their start and end apart: 2 -> 0, of which waited for: 1 -> 0; matrix products, arithmetic and copies ran while one was open for 1% -> 0% of each run, Pallas kernels for 0% -> 0%
where the time goes in v1:
time: 101 us
  Pallas kernels  95.7 us (95%)
  local copies, waits for them, and re-layouts  4.15 us (4%)
    pallas_call x1, Pallas kernels, layer(): pl.pallas_call(functools.partial(layer_kernel, ep_count, tp_count, slots)...  95.7 us
    unnamed x2, local copies, waits for them, and re-layouts  3.55 us

profile of v1, /device:TPU:1, one launch (start us, length us, event | category | flops | bytes accessed | tf_op | source)
XLA Modules:
  0.0 100.5 jit_solution(14364423754505247313)
XLA Ops:
  0.7 0.6 broadcast_in_dim_tile.3.inverse
  1.2 95.7 %layer.1 = (bf16[128,2048]{1,0:T(8,128)(2,1)}, bf16[512,256]{1,0:T(8,128)(2,1)}) custom-call(bf16[128,2048]{1,0:T(8,128)(2,1)} %second_in.1, f32[1,2048]{1,0:T(1,128)} %bitcast.6, f32[1,2048]{1,0:T(1,128)} %bitcast.7, bf16[16,2048]{1,0:T(8,128)(2,1)} %bitcast.5, s32[4,128]{1,0:T(4,128)} %bitcast.8, f32[1,128]{1,0:T(1,128)} %broadcast_in_dim_tile.3.inverse, ...), custom_call_target="tpu_custom_call" | custom-call | tf_op jit(solution)/shard_map/layer/pallas_call | solution.py:630
  97.0 1.7 %copy.20 = bf16[512,256]{1,0:T(8,128)(2,1)} copy(bf16[512,256]{1,0:T(8,128)(2,1)} %get-tuple-element.8) | data formatting | bytes 524288
  98.7 1.9 %copy.21 = bf16[128,2048]{1,0:T(8,128)(2,1)} copy(bf16[128,2048]{1,0:T(8,128)(2,1)} %get-tuple-element.9) | data formatting | bytes 1048576
  (2 shorter events, 0.0 us)

commit v2 on v1

--- a/solution.py
+++ b/solution.py
@@ -2,6 +2,7 @@
 
 import jax
 import jax.numpy as jnp
+import numpy as np
 from jax import lax
 from jax.experimental import pallas as pl
 from jax.experimental.pallas import tpu as pltpu
@@ -14,6 +15,7 @@
 ROUTED_SCALE = 2.5
 LANES = 128
 CHUNK = 512
+LAG = 2
 MESH = pl.DeviceIdType.MESH
 VMEM_LIMIT = 63 * 2**20
 
@@ -87,10 +89,10 @@
     barrier = greet(grp, ep, tp, ep_count, tp_count)
 
     def toward(side):
-        return (grp, ep, tp + (1 if side == 0 else -1))
+        return (grp, ep, tp + 1 - 2 * side)
 
     def exists(side):
-        return tp < tp_count - 1 if side == 0 else tp > 0
+        return (tp + 1 - 2 * side >= 0) & (tp + 1 - 2 * side < tp_count)
 
     def peer(d):
         return (grp, lax.rem(ep + d, ep_count), tp)
@@ -105,9 +107,25 @@
 
         lax.fori_loop(0, count, step, 0)
 
-    def at(side, distance):
-        block = tp - distance if side == 0 else tp + distance
-        return block, (block >= 0 if side == 0 else block < tp_count)
+    def near(side, distance):
+        block = tp + (2 * side - 1) * distance
+        return block, (block >= 0) & (block < tp_count)
+
+    swaps = tp_count > 2
+
+    def swapped(side, block, allowed):
+        far, second = (tp_count - 1) * side, 1 + (tp_count - 3) * side
+        other = jnp.where(block == second, far, jnp.where(block == far, second, block))
+        return jnp.where(allowed, other, block)
+
+    def at(side, order):
+        block, inside = near(side, order)
+        if swaps:
+            block = swapped(side, block, jnp.where(side == 0, tp, tp_count - 1 - tp) >= 2)
+        return block, inside
+
+    def late(side):
+        return (tp == 1 + side * (tp_count - 3)) & swaps
 
     def send_second(side, block, part):
         ref = gath2.at[block, :, part_span(part)]
@@ -217,11 +235,11 @@
 
         each_part(columns)
 
-    def experts_at(distance):
+    def experts_at(order):
         def one(side, carry):
-            block = tp + (2 * side - 1) * distance
-
-            @pl.when((block >= 0) & (block < tp_count) & ((distance > 0) | (side == 0)))
+            block, inside = at(side, order)
+
+            @pl.when(inside & ((order > 0) | (side == 0)))
             def _():
                 expert(block)
 
@@ -244,14 +262,14 @@
             piece = values[:, start : start + size]
             if size == LANES:
                 lane = lax.broadcasted_iota(jnp.int32, piece.shape, 1)
-                swapped = jnp.where(
+                crossed = jnp.where(
                     lax.rem(lane, HEAD_DIM) < half,
                     pltpu.roll(piece, LANES - half, 1),
                     pltpu.roll(piece, half, 1),
                 )
             else:
-                swapped = jnp.concatenate([piece[:, half:], piece[:, :half]], axis=1)
-            pieces.append(piece * cos_rows[:, :size] + swapped * sin_rows[:, :size])
+                crossed = jnp.concatenate([piece[:, half:], piece[:, :half]], axis=1)
+            pieces.append(piece * cos_rows[:, :size] + crossed * sin_rows[:, :size])
         return pieces[0] if len(pieces) == 1 else jnp.concatenate(pieces, axis=1)
 
     def project(block):
@@ -329,7 +347,7 @@
     def send_own(part):
         for side in range(2):
 
-            @pl.when(exists(side))
+            @pl.when(exists(side) & jnp.logical_not(late(side)))
             def _():
                 send_second(side, tp, part).start()
 
@@ -398,9 +416,13 @@
         )
 
     def reduce_step(step):
-        for side in range(2):
-            block = step - tp if side == 0 else 2 * (tp_count - 1) - step - tp
-            active = (block > tp) & (block < tp_count) if side == 0 else (block < tp) & (block >= 0)
+        def one(turn, carry):
+            side = jnp.where(2 * tp < tp_count, 1 - turn, turn)
+            block = jnp.where(side == 0, step - tp, 2 * (tp_count - 1) - step - tp)
+            active = (block >= 0) & (block < tp_count)
+            if swaps:
+                block = swapped(1 - side, block, True)
+            active = active & ((block - tp) * (1 - 2 * side) > 0)
 
             @pl.when(active)
             def _():
@@ -411,7 +433,7 @@
                     return_part(block, part).wait_recv()
                     own = value_of(block, weights, span)
 
-                    @pl.when(tp > 0 if side == 0 else tp < tp_count - 1)
+                    @pl.when(exists(1 - side))
                     def _():
                         pass_on(side, block, part).wait_recv()
 
@@ -420,14 +442,21 @@
 
                 each_part(one_part)
 
+            return carry
+
+        lax.fori_loop(0, 2, one, 0)
+
     early = tp_count > 2
+    ends = (tp == 0) | (tp == tp_count - 1)
 
     def hop(k, carry):
-        def one_part(part):
-            for side in range(2):
+        def one_turn(turn):
+            def receive(second, carry):
+                part = turn - second * LAG
+                side = jnp.where(2 * tp < tp_count, second, 1 - second)
                 block, inside = at(side, k)
 
-                @pl.when(inside)
+                @pl.when(inside & (part >= 0) & (part < parts))
                 def _():
                     send_second(side, block, part).wait_recv()
 
@@ -443,14 +472,40 @@
                         def _():
                             send_meta(side, block).start()
 
-            for side in range(2):
-                block, inside = at(side, k)
-
-                @pl.when(inside)
+                    @pl.when(late(side) & (k == 1) & (part == parts - 1))
+                    def _():
+                        for own in range(parts):
+                            send_second(side, tp, own).start()
+
+                    pick_part(block, part)
+
+                return carry
+
+            lax.fori_loop(0, 2, receive, 0)
+
+            @pl.when(k == 1)
+            def _():
+                @pl.when(turn == 1)
                 def _():
-                    pick_part(block, part)
-
-        each_part(one_part)
+                    tables()
+
+                @pl.when(turn == 2)
+                def _():
+                    project(tp)
+
+            if early:
+
+                @pl.when(ends & (k == tp_count - 1) & (turn == LAG + 1))
+                def _():
+                    reduce_step(1)
+
+            inner = ends & (k > 1) & (k < tp_count - 1) & (turn == LAG + 1)
+
+            @pl.when(inner | ((k == 1) & (turn == LAG + 2)))
+            def _():
+                experts_at(k - 1)
+
+        each_part(one_turn, parts + LAG)
         for side in range(2):
             start_own_first(side, k)
         for side in range(2):
@@ -460,22 +515,15 @@
             def _():
                 shared_hidden(block)
 
-        if early:
-
-            @pl.when(k == tp_count - 1)
-            def _():
-                reduce_step(1)
-
-        experts_at(k - 1)
-
-        @pl.when(k == 1)
+        @pl.when((k > 1) & (jnp.logical_not(ends) | (k == tp_count - 1)))
         def _():
-            tables()
-            project(tp)
+            experts_at(k - 1)
 
         return carry
 
     lax.fori_loop(1, tp_count, hop, 0)
+    if early:
+        reduce_step(2)
     experts_at(tp_count - 1)
     for part in range(parts):
         for d in range(1, ep_count):
@@ -499,16 +547,23 @@
 
     def first_hop(k, carry):
         for side in range(2):
-            block, inside = at(side, k)
+            block, inside = near(side, k)
 
             @pl.when(inside & exists(side))
             def _():
                 send_first(side, block).wait_recv()
                 send_first(side, block).start()
 
-        reduce_step(jnp.where(k == 1, 2 if early else 1, 2 * k - 1))
+        if early:
+
+            @pl.when(k > 1)
+            def _():
+                reduce_step(2 * k - 1)
+
+        else:
+            reduce_step(2 * k - 1)
         for side in range(2):
-            block, inside = at(side, k)
+            block, inside = near(side, k)
 
             @pl.when(inside & jnp.logical_not(exists(side)))
             def _():
@@ -711,10 +766,10 @@
     capacity = 3 * top_count * tokens // (2 * experts)
     slots = -(-capacity // 16) * 16
     half = HEAD_DIM // 2
-    inverse = THETA ** (-(jnp.arange(half, dtype=jnp.float32) * 2.0) / HEAD_DIM)
+    inverse = np.float32(THETA) ** (-(np.arange(half, dtype=np.float32) * np.float32(2.0)) / np.float32(HEAD_DIM))
     moe_out, mixed = layer(
         moe_in, mixer_in, moe_gain[None, :], mixer_gain[None, :], router.T, routes.T,
-        jnp.tile(inverse, LANES // half)[None, :], sink_logit[None, :],
+        jnp.asarray(np.tile(inverse, LANES // half)[None, :]), sink_logit[None, :],
         expert_gate, expert_up, expert_down, shared_gate, shared_up, shared_down,
         w_query, w_key, w_value, ep_count, tp_count, slots,
     )

time: 101 us -> 93.2 us (0.923)
  Pallas kernels: 95.7 us -> 88.2 us
    pallas_call x1, Pallas kernels: 95.7 us -> 88.2 us  [layer(): pl.pallas_call(functools.partial(layer_kernel, ep_count, tp_count, slots)...]
where the time goes in v2:
time: 93.2 us; the launch traced here: 92.4 us
  Pallas kernels  88.2 us (95%)
  local copies, waits for them, and re-layouts  3.55 us (4%)
    pallas_call x1, Pallas kernels, layer(): pl.pallas_call(functools.partial(layer_kernel, ep_count, tp_count, slots)...  88.2 us
    unnamed x2, local copies, waits for them, and re-layouts  3.55 us

profile of v2, /device:TPU:1, one launch (start us, length us, event | category | flops | bytes accessed | tf_op | source)
XLA Modules:
  0.0 92.4 jit_solution(3016549155457063366)
XLA Ops:
  0.6 88.2 %layer.1 = (bf16[128,2048]{1,0:T(8,128)(2,1)}, bf16[512,256]{1,0:T(8,128)(2,1)}) custom-call(bf16[128,2048]{1,0:T(8,128)(2,1)} %second_in.1, f32[1,2048]{1,0:T(1,128)} %bitcast.6, f32[1,2048]{1,0:T(1,128)} %bitcast.7, bf16[16,2048]{1,0:T(8,128)(2,1)} %bitcast.5, s32[4,128]{1,0:T(4,128)} %bitcast.8, f32[1,128]{1,0:T(1,128)} %constant.2.clone.inverse, ...), custom_call_target="tpu_custom_call" | custom-call | tf_op jit(solution)/shard_map/layer/pallas_call | solution.py:685
  88.8 1.7 %copy.21 = bf16[512,256]{1,0:T(8,128)(2,1)} copy(bf16[512,256]{1,0:T(8,128)(2,1)} %get-tuple-element.8) | data formatting | bytes 524288
  90.5 1.9 %copy.22 = bf16[128,2048]{1,0:T(8,128)(2,1)} copy(bf16[128,2048]{1,0:T(8,128)(2,1)} %get-tuple-element.9) | data formatting | bytes 1048576

commit v3 on v2

--- a/solution.py
+++ b/solution.py
@@ -53,11 +53,11 @@
     ep_count, tp_count, slots,
     second_in, gain_second, gain_first, router, routes, inverse, sink,
     first_hbm, gate_hbm, up_hbm, down_hbm, sgate_hbm, sup_hbm, sdown_hbm, wq_hbm, wk_hbm, wv_hbm,
-    out, mixed,
-    gath2, gath1, first_in, metag, sbuf, disp, back, sides, psend,
+    out, mixed_out,
+    mixed, gath2, gath1, first_in, metag, sbuf, disp, back, sides, psend,
     gate, up, down, sgate, sup, sdown, wq, wk, wv,
     hidden, hexp, cosine, sine, qbuf, kvbuf,
-    l_sem, s2, r2, sm, rm, s1, r1, sd, rd, sb, rb, sp, rs, hs, hr,
+    l_sem, s2, r2, sm, rm, s1, r1, sd, rd, sb, rb, sp, rs, hs, hr, out_sem, mixed_sem,
 ):
     grp, ep, tp = lax.axis_index("grp"), lax.axis_index("ep"), lax.axis_index("tp")
     rows, width = second_in.shape
@@ -175,6 +175,14 @@
             hs.at[side], hr.at[side], (grp, ep + (1 if side == 0 else -1), tp),
         )
 
+    def out_copy(part):
+        span = part_span(part)
+        return pltpu.make_async_copy(psend.at[tp, :, span], out.at[:, span], out_sem.at[part])
+
+    def mixed_copy(block):
+        span = part_span(block, rows)
+        return pltpu.make_async_copy(mixed.at[span], mixed_out.at[span], mixed_sem.at[block])
+
     def normalize(source, gain, target):
         def squares(part, carry):
             values = source[:, part_span(part)].astype(f32)
@@ -283,6 +291,15 @@
         kvbuf[pl.ds(pl.multiple_of(base + rows, rows), rows), :] = jnp.concatenate(
             [rotated(key, cos_rows, sin_rows), value], axis=1
         ).astype(bf16)
+
+    def start_halo(block):
+        @pl.when((block == tp_count - 1) & (ep < ep_count - 1))
+        def _():
+            halo(0).start()
+
+        @pl.when((block == 0) & (ep > 0))
+        def _():
+            halo(1).start()
 
     def tables():
         def one(block):
@@ -329,6 +346,7 @@
                 share = (weights * (1.0 / summed)).astype(bf16)
                 pieces.append(jnp.dot(share, values, preferred_element_type=f32))
         mixed[pl.ds(base, rows), :] = jnp.concatenate(pieces, axis=1).astype(bf16)
+        mixed_copy(block).start()
 
     normalize(second_in, gain_second, gath2.at[tp])
     ids = lax.broadcasted_iota(jnp.int32, (experts, rows), 0)
@@ -492,6 +510,7 @@
                 @pl.when(turn == 2)
                 def _():
                     project(tp)
+                    start_halo(tp)
 
             if early:
 
@@ -522,28 +541,16 @@
         return carry
 
     lax.fori_loop(1, tp_count, hop, 0)
+    experts_at(tp_count - 1)
+
+    def give_back(low, high):
+        for part in range(low, high):
+            for d in range(1, ep_count):
+                return_copy(tp, d, part).start()
+
+    give_back(0, parts // 2)
     if early:
         reduce_step(2)
-    experts_at(tp_count - 1)
-    for part in range(parts):
-        for d in range(1, ep_count):
-            return_copy(tp, d, part).start()
-
-    def start_halo(block):
-        @pl.when((block == tp_count - 1) & (ep < ep_count - 1))
-        def _():
-            halo(0).start()
-
-        @pl.when((block == 0) & (ep > 0))
-        def _():
-            halo(1).start()
-
-    start_halo(tp)
-
-    def attend_inner(block):
-        @pl.when((block > 0) & (block < tp_count - 1))
-        def _():
-            attend(block)
 
     def first_hop(k, carry):
         for side in range(2):
@@ -581,6 +588,10 @@
 
         lax.fori_loop(0, 2, use, 0)
 
+        @pl.when(k == jnp.maximum(tp, tp_count - 1 - tp))
+        def _():
+            give_back(parts // 2, parts)
+
         def settle(side, carry):
             block = tp + (2 * side - 1) * (k - 1)
 
@@ -592,22 +603,6 @@
 
         lax.fori_loop(0, 2, settle, 0)
 
-        @pl.when(k == jnp.maximum(tp, tp_count - 1 - tp))
-        def _():
-            @pl.when(ep < ep_count - 1)
-            def _():
-                halo(1).wait_recv()
-
-            @pl.when(ep > 0)
-            def _():
-                halo(0).wait_recv()
-
-            def edge(side, carry):
-                attend((tp_count - 1) * (1 - side))
-                return carry
-
-            lax.fori_loop(0, 2, edge, 0)
-
         if early:
 
             @pl.when(k > 1)
@@ -617,6 +612,20 @@
         return carry
 
     lax.fori_loop(1, tp_count, first_hop, 0)
+
+    @pl.when(ep < ep_count - 1)
+    def _():
+        halo(1).wait_recv()
+
+    @pl.when(ep > 0)
+    def _():
+        halo(0).wait_recv()
+
+    def edge(side, carry):
+        attend((tp_count - 1) * (1 - side))
+        return carry
+
+    lax.fori_loop(0, 2, edge, 0)
     own_weights = weights_of(tp)
 
     def last_part(part):
@@ -632,9 +641,10 @@
         def _():
             pass_on(1, tp, part).wait_recv()
 
-        out[:, span] = (
+        psend[tp, :, span] = (
             own + sides[0, tp, :, span].astype(f32) + sides[1, tp, :, span].astype(f32)
         ).astype(bf16)
+        out_copy(part).start()
 
     each_part(last_part)
 
@@ -657,6 +667,8 @@
                     pass_on(side, block, part).wait_send()
 
     each_part(finish, tp_count)
+    each_part(lambda part: out_copy(part).wait())
+    each_part(lambda block: mixed_copy(block).wait(), tp_count)
 
     @pl.when(ep < ep_count - 1)
     def _():
@@ -689,8 +701,9 @@
             jax.ShapeDtypeStruct((span, wq.shape[1]), bf16),
         ),
         in_specs=[vmem] * 6 + [smem] + [hbm] * 10,
-        out_specs=(vmem, vmem),
+        out_specs=(hbm, hbm),
         scratch_shapes=[
+            pltpu.VMEM((span, wq.shape[1]), bf16),
             pltpu.VMEM((tp_count, rows, width), bf16),
             pltpu.VMEM((tp_count, rows, width), bf16),
             pltpu.VMEM((rows, width), bf16),
@@ -730,6 +743,8 @@
             dma((2, tp_count, parts)),
             dma((2,)),
             dma((2,)),
+            dma((parts,)),
+            dma((tp_count,)),
         ],
         compiler_params=pltpu.CompilerParams(
             collective_id=0, has_side_effects=True, vmem_limit_bytes=VMEM_LIMIT
@@ -739,6 +754,45 @@
         second, gain_second, gain_first, router, routes, inverse, sink,
         first, gate, up, down, sgate, sup, sdown, wq, wk, wv,
     )
+
+
+def settle_kernel(first, second, first_out, second_out, first_buf, second_buf, sems):
+    arrays = [(first, first_buf, first_out), (second, second_buf, second_out)]
+    pieces = []
+    for i, (source, buffer, target) in enumerate(arrays):
+        half = source.shape[0] // 2
+        for j in range(2):
+            rows = pl.ds(j * half, half)
+            pieces.append(
+                (
+                    pltpu.make_async_copy(source.at[rows], buffer.at[rows], sems.at[0, i, j]),
+                    pltpu.make_async_copy(buffer.at[rows], target.at[rows], sems.at[1, i, j]),
+                )
+            )
+    for load, _ in pieces:
+        load.start()
+    for load, store in pieces:
+        load.wait()
+        store.start()
+    for _, store in pieces:
+        store.wait()
+
+
+def settle(first, second):
+    hbm = pl.BlockSpec(memory_space=pl.ANY)
+    return pl.pallas_call(
+        settle_kernel,
+        out_shape=(jax.ShapeDtypeStruct(first.shape, first.dtype), jax.ShapeDtypeStruct(second.shape, second.dtype)),
+        in_specs=[hbm, hbm],
+        out_specs=(hbm, hbm),
+        scratch_shapes=[
+            pltpu.VMEM(first.shape, first.dtype),
+            pltpu.VMEM(second.shape, second.dtype),
+            pltpu.SemaphoreType.DMA((2, 2, 2)),
+        ],
+        compiler_params=pltpu.CompilerParams(vmem_limit_bytes=VMEM_LIMIT),
+        name="settle",
+    )(first, second)
 
 
 def body(
@@ -773,6 +827,7 @@
         expert_gate, expert_up, expert_down, shared_gate, shared_up, shared_down,
         w_query, w_key, w_value, ep_count, tp_count, slots,
     )
+    moe_out, mixed = settle(moe_out, mixed)
     return (mixed, moe_out)
 
 

time: 93.2 us -> 91.2 us (0.979)
  local copies, waits for them, and re-layouts: 3.55 us -> 0 us
  Pallas kernels: 88.2 us -> 89.2 us
    unnamed x2 -> x0, local copies, waits for them, and re-layouts: 3.55 us -> none
    pallas_call x0 -> x1, Pallas kernels: none -> 1.89 us  [settle(): pl.pallas_call(settle_kernel, out_shape=(jax.ShapeDtypeStruct(first.shape...]
where the time goes in v3:
time: 91.2 us; the launch traced here: 89.8 us
  Pallas kernels  89.2 us (98%)
    pallas_call x1, Pallas kernels, layer(): pl.pallas_call(functools.partial(layer_kernel, ep_count, tp_count, slots)...  87.3 us
    pallas_call x1, Pallas kernels, settle(): pl.pallas_call(settle_kernel, out_shape=(jax.ShapeDtypeStruct(first.shape...  1.89 us

profile of v3, /device:TPU:1, one launch (start us, length us, event | category | flops | bytes accessed | tf_op | source)
XLA Modules:
  0.0 89.8 jit_solution(5236401876074040798)
XLA Ops:
  0.6 87.3 %layer.1 = (bf16[128,2048]{1,0:T(8,128)(2,1)}, bf16[512,256]{1,0:T(8,128)(2,1)}) custom-call(bf16[128,2048]{1,0:T(8,128)(2,1)} %second_in.1, f32[1,2048]{1,0:T(1,128)} %bitcast.6, f32[1,2048]{1,0:T(1,128)} %bitcast.7, bf16[16,2048]{1,0:T(8,128)(2,1)} %bitcast.5, s32[4,128]{1,0:T(4,128)} %bitcast.8, f32[1,128]{1,0:T(1,128)} %constant.2.clone.inverse, ...), custom_call_target="tpu_custom_call" | custom-call | tf_op jit(solution)/shard_map/layer/pallas_call | solution.py:697
  87.9 1.9 %settle.1 = (bf16[128,2048]{1,0:T(8,128)(2,1)}, bf16[512,256]{1,0:T(8,128)(2,1)}) custom-call(bf16[128,2048]{1,0:T(8,128)(2,1)} %get-tuple-element.6.first, bf16[512,256]{1,0:T(8,128)(2,1)} %get-tuple-element.7.second), custom_call_target="tpu_custom_call" | custom-call | tf_op jit(solution)/shard_map/settle/pallas_call | solution.py:783

commit v4 on v3

--- a/solution.py
+++ b/solution.py
@@ -31,7 +31,7 @@
     )
 
 
-def greet(grp, ep, tp, ep_count, tp_count):
+def greet(grp, ep, tp, grp_count, ep_count, tp_count):
     barrier = pltpu.get_barrier_semaphore()
 
     @pl.when(tp > 0)
@@ -46,18 +46,22 @@
         pl.semaphore_signal(
             barrier, inc=1, device_id=(grp, lax.rem(ep + d, ep_count), tp), device_id_type=MESH
         )
+    for d in range(1, grp_count):
+        pl.semaphore_signal(
+            barrier, inc=1, device_id=(lax.rem(grp + d, grp_count), ep, tp), device_id_type=MESH
+        )
     return barrier
 
 
 def layer_kernel(
-    ep_count, tp_count, slots,
+    grp_count, ep_count, tp_count, slots,
     second_in, gain_second, gain_first, router, routes, inverse, sink,
     first_hbm, gate_hbm, up_hbm, down_hbm, sgate_hbm, sup_hbm, sdown_hbm, wq_hbm, wk_hbm, wv_hbm,
     out, mixed_out,
     mixed, gath2, gath1, first_in, metag, sbuf, disp, back, sides, psend,
-    gate, up, down, sgate, sup, sdown, wq, wk, wv,
+    gate, up, down, sgate, sup, sdown, wq, wk, wv, far_q, far_k, far_v, lent_q, lent_kv,
     hidden, hexp, cosine, sine, qbuf, kvbuf,
-    l_sem, s2, r2, sm, rm, s1, r1, sd, rd, sb, rb, sp, rs, hs, hr, out_sem, mixed_sem,
+    l_sem, s2, r2, sm, rm, s1, r1, sd, rd, sb, rb, sp, rs, hs, hr, out_sem, mixed_sem, ws, wr, qs, qr,
 ):
     grp, ep, tp = lax.axis_index("grp"), lax.axis_index("ep"), lax.axis_index("tp")
     rows, width = second_in.shape
@@ -86,7 +90,7 @@
     ]
     for copy in local:
         copy.start()
-    barrier = greet(grp, ep, tp, ep_count, tp_count)
+    barrier = greet(grp, ep, tp, grp_count, ep_count, tp_count)
 
     def toward(side):
         return (grp, ep, tp + 1 - 2 * side)
@@ -133,6 +137,86 @@
 
     def send_meta(side, block):
         return remote(metag.at[block], metag.at[block], sm.at[side, block], rm.at[block], toward(side))
+
+    assist = tp_count >= 4
+    ends = (tp == 0) | (tp == tp_count - 1)
+    slim = tp_count == 4
+    plain = jnp.logical_not(ends) | (not assist)
+    helps = ((tp == 1) | (tp == tp_count - 2)) & assist
+    outward = jnp.where(tp == 1, 1, 0)
+    pair = 2 if ep_count % 2 == 0 else 1
+    core = lax.rem(ep, pair)
+    piece_rows = width // (grp_count * pair)
+    lent = [(wq, far_q), (wk, far_k), (wv, far_v)]
+
+    def carries(side):
+        target = tp + 1 - 2 * side
+        return exists(side) & (((target > 0) & (target < tp_count - 1)) | (not assist))
+
+    def share_of(group, half):
+        return group * pair + half
+
+    def lend(share, to, device, own):
+        span = pl.ds(pl.multiple_of(share * piece_rows, piece_rows), piece_rows)
+        return [
+            remote(
+                (near_ref if own else far_ref).at[span], far_ref.at[span],
+                ws.at[share, to, i], wr.at[share, i], device,
+            )
+            for i, (near_ref, far_ref) in enumerate(lent)
+        ]
+
+    def lend_out():
+        return lend(share_of(grp, core), 0, (grp, ep, jnp.where(tp == 0, 1, tp_count - 2)), True)
+
+    def partner():
+        return (grp, ep + 1 - 2 * core, tp)
+
+    def relays():
+        mine = share_of(grp, core)
+        copies = []
+        for d in range(1, grp_count):
+            copies.append(lend(mine, d, (lax.rem(grp + d, grp_count), ep, tp), False))
+        if pair == 2:
+            copies.append(lend(mine, 0, partner(), False))
+        return copies
+
+    def relays_across():
+        copies = []
+        for d in range(1, grp_count):
+            copies.append(lend(share_of(lax.rem(grp + d, grp_count), core), 0, partner(), False))
+        return copies
+
+    def relay_first():
+        for copy in lend(share_of(grp, core), 0, toward(outward), False):
+            copy.wait_recv()
+        for copies in relays():
+            for copy in copies:
+                copy.start()
+
+    def relay_second():
+        for copies in relays_across():
+            for copy in copies:
+                copy.wait_recv()
+            if pair == 2:
+                for copy in copies:
+                    copy.start()
+
+    def relay_last():
+        if pair == 2:
+            for group in range(grp_count):
+                for copy in lend(share_of(group, 1 - core), 0, partner(), False):
+                    copy.wait_recv()
+
+    def query_copy(block, device):
+        return remote(
+            lent_q.at[block], qbuf.at[part_span(block, rows)], qs.at[0, block], qr.at[0, block], device
+        )
+
+    def kv_copy(block, device):
+        return remote(
+            lent_kv.at[block], kvbuf.at[part_span(block + 1, rows)], qs.at[1, block], qr.at[1, block], device
+        )
 
     def send_first(side, block):
         return remote(gath1.at[block], gath1.at[block], s1.at[side, block], r1.at[block], toward(side))
@@ -258,7 +342,7 @@
     def start_own_first(side, step):
         last = tp if side == 0 else tp_count - 1 - tp
 
-        @pl.when(exists(side) & (step == last))
+        @pl.when(carries(side) & (step == last))
         def _():
             send_first(side, tp).start()
 
@@ -280,17 +364,23 @@
             pieces.append(piece * cos_rows[:, :size] + crossed * sin_rows[:, :size])
         return pieces[0] if len(pieces) == 1 else jnp.concatenate(pieces, axis=1)
 
+    def projected(block, query_w, key_w, value_w):
+        span = part_span(block, rows)
+        values = gath1[block]
+        cos_rows, sin_rows = cosine[span, :], sine[span, :]
+        query = jnp.dot(values, query_w[...], preferred_element_type=f32)
+        key = jnp.dot(values, key_w[...], preferred_element_type=f32)
+        value = jnp.dot(values, value_w[...], preferred_element_type=f32)
+        joined = jnp.concatenate([rotated(key, cos_rows, sin_rows), value], axis=1).astype(bf16)
+        return rotated(query, cos_rows, sin_rows).astype(bf16), joined
+
     def project(block):
-        base = pl.multiple_of(block * rows, rows)
-        values = gath1[block]
-        cos_rows, sin_rows = cosine[pl.ds(base, rows), :], sine[pl.ds(base, rows), :]
-        query = jnp.dot(values, wq[...], preferred_element_type=f32)
-        key = jnp.dot(values, wk[...], preferred_element_type=f32)
-        value = jnp.dot(values, wv[...], preferred_element_type=f32)
-        qbuf[pl.ds(base, rows), :] = rotated(query, cos_rows, sin_rows).astype(bf16)
-        kvbuf[pl.ds(pl.multiple_of(base + rows, rows), rows), :] = jnp.concatenate(
-            [rotated(key, cos_rows, sin_rows), value], axis=1
-        ).astype(bf16)
+        qbuf[part_span(block, rows), :], kvbuf[part_span(block + 1, rows), :] = projected(block, wq, wk, wv)
+
+    def project_far(block):
+        lent_q[block], lent_kv[block] = projected(block, far_q, far_k, far_v)
+        query_copy(block, toward(outward)).start()
+        kv_copy(block, toward(outward)).start()
 
     def start_halo(block):
         @pl.when((block == tp_count - 1) & (ep < ep_count - 1))
@@ -361,7 +451,8 @@
         preferred_element_type=f32,
     )
     metag[tp, 0:experts, :] = jnp.where(hit, before, -1.0)
-    pl.semaphore_wait(barrier, ep_count + jnp.where((tp > 0) & (tp < tp_count - 1), 1, 0))
+    pl.semaphore_wait(barrier, ep_count + grp_count - 1 + jnp.where((tp > 0) & (tp < tp_count - 1), 1, 0))
+
     def send_own(part):
         for side in range(2):
 
@@ -392,8 +483,6 @@
     lax.fori_loop(1, parts, pick_rest, 0)
     local[0].wait()
     normalize(first_in, gain_first, gath1.at[tp])
-    for side in range(2):
-        start_own_first(side, 0)
 
     @pl.when(tp == 0)
     def _():
@@ -413,6 +502,15 @@
 
     for copy in local[1:]:
         copy.wait()
+    if assist:
+
+        @pl.when(ends)
+        def _():
+            for copy in lend_out():
+                copy.start()
+
+    for side in range(2):
+        start_own_first(side, 0)
     shared_hidden(tp)
 
     def weights_of(block):
@@ -433,6 +531,57 @@
             + jnp.dot(hidden[block], sdown[:, span], preferred_element_type=f32)
         )
 
+    def reduce_piece(side, block, part, weights):
+        span = part_span(part)
+        return_part(block, part).wait_recv()
+        own = value_of(block, weights, span)
+
+        @pl.when(exists(1 - side))
+        def _():
+            pass_on(side, block, part).wait_recv()
+
+        psend[block, :, span] = (own + sides[side, block, :, span].astype(f32)).astype(bf16)
+        pass_on(side, block, part).start()
+
+    def edge(last):
+        @pl.when((last == 1) & (ep < ep_count - 1))
+        def _():
+            halo(1).wait_recv()
+
+        @pl.when((last == 0) & (ep > 0))
+        def _():
+            halo(0).wait_recv()
+
+        attend((tp_count - 1) * last)
+
+    def reduce_merged():
+        end = (tp_count - 1) * (1 - outward)
+        second = 1 + (tp_count - 3) * outward
+
+        def slot(i):
+            def stream(j, carry):
+                part = i - LAG * j
+                side = jnp.where(j == 1, outward, 1 - outward)
+                block = jnp.where(j == 0, tp_count - 1 - end, jnp.where(j == 1, end, second))
+
+                @pl.when((part >= 0) & (part < parts))
+                def _():
+                    reduce_piece(side, block, part, weights_of(block))
+
+                return carry
+
+            lax.fori_loop(0, 3, stream, 0)
+
+            @pl.when(i == 0)
+            def _():
+                attend(second)
+
+            @pl.when((i == 3) | (i == 5))
+            def _():
+                edge(jnp.where(i == 3, 1, 0))
+
+        each_part(slot, parts + 2 * LAG)
+
     def reduce_step(step):
         def one(turn, carry):
             side = jnp.where(2 * tp < tp_count, 1 - turn, turn)
@@ -445,27 +594,13 @@
             @pl.when(active)
             def _():
                 weights = weights_of(block)
-
-                def one_part(part):
-                    span = part_span(part)
-                    return_part(block, part).wait_recv()
-                    own = value_of(block, weights, span)
-
-                    @pl.when(exists(1 - side))
-                    def _():
-                        pass_on(side, block, part).wait_recv()
-
-                    psend[block, :, span] = (own + sides[side, block, :, span].astype(f32)).astype(bf16)
-                    pass_on(side, block, part).start()
-
-                each_part(one_part)
+                each_part(lambda part: reduce_piece(side, block, part, weights))
 
             return carry
 
         lax.fori_loop(0, 2, one, 0)
 
     early = tp_count > 2
-    ends = (tp == 0) | (tp == tp_count - 1)
 
     def hop(k, carry):
         def one_turn(turn):
@@ -518,9 +653,15 @@
                 def _():
                     reduce_step(1)
 
-            inner = ends & (k > 1) & (k < tp_count - 1) & (turn == LAG + 1)
-
-            @pl.when(inner | ((k == 1) & (turn == LAG + 2)))
+            if assist:
+
+                @pl.when(helps & (k == 2) & (turn == LAG + 1))
+                def _():
+                    relay_first()
+
+            middle = ends & (k > 1) & (k == tp_count - 1) & (turn == LAG)
+
+            @pl.when(middle | ((k == 1) & (turn == LAG + 2)))
             def _():
                 experts_at(k - 1)
 
@@ -534,13 +675,27 @@
             def _():
                 shared_hidden(block)
 
-        @pl.when((k > 1) & (jnp.logical_not(ends) | (k == tp_count - 1)))
+        if slim:
+
+            @pl.when(helps & (k == tp_count - 1))
+            def _():
+                side = 1 - outward
+                block, _ = near(side, 1)
+                send_first(side, block).wait_recv()
+                send_first(side, block).start()
+                project(block)
+                start_halo(block)
+
+        @pl.when((k > 1) & (jnp.logical_not(ends) | (k < tp_count - 1)))
         def _():
             experts_at(k - 1)
 
         return carry
 
     lax.fori_loop(1, tp_count, hop, 0)
+    if early:
+        reduce_step(2)
+
     experts_at(tp_count - 1)
 
     def give_back(low, high):
@@ -548,84 +703,125 @@
             for d in range(1, ep_count):
                 return_copy(tp, d, part).start()
 
-    give_back(0, parts // 2)
-    if early:
-        reduce_step(2)
+    @pl.when(ends | (not slim))
+    def _():
+        give_back(0, parts // 2)
+
+    if assist:
+
+        @pl.when(helps)
+        def _():
+            relay_second()
+
 
     def first_hop(k, carry):
+        def open_at(side):
+            block, inside = near(side, k)
+            if slim:
+                inside = inside & ((k > 1) | (side == outward))
+            return block, inside
+
         for side in range(2):
-            block, inside = near(side, k)
-
-            @pl.when(inside & exists(side))
+            block, inside = open_at(side)
+
+            @pl.when(inside & plain)
             def _():
                 send_first(side, block).wait_recv()
-                send_first(side, block).start()
-
-        if early:
+
+                @pl.when(carries(side))
+                def _():
+                    send_first(side, block).start()
+
+        if assist:
+
+            @pl.when(helps)
+            def _():
+                @pl.when(k == 1)
+                def _():
+                    relay_last()
+
+                def one(turn, carry):
+                    block, inside = near(outward, k * turn)
+
+                    @pl.when(inside & ((turn == 1) | (k == 1)))
+                    def _():
+                        project_far(block)
+
+                    return carry
+
+                lax.fori_loop(0, 2, one, 0)
+
+        def use(side, carry):
+            block, inside = open_at(side)
+
+            @pl.when(inside & plain)
+            def _():
+                project(block)
+                start_halo(block)
+
+            return carry
+
+        lax.fori_loop(0, 2, use, 0)
+        @pl.when((k == jnp.maximum(tp, tp_count - 1 - tp)) & plain)
+        def _():
+            give_back(0 if slim else parts // 2, parts)
+
+        if slim:
+
+            @pl.when((k == 2) & ends)
+            def _():
+                reduce_step(3)
+
+            @pl.when((k == 2) & helps)
+            def _():
+                reduce_merged()
+
+        elif early:
 
             @pl.when(k > 1)
             def _():
                 reduce_step(2 * k - 1)
+                reduce_step(2 * k)
 
         else:
             reduce_step(2 * k - 1)
-        for side in range(2):
-            block, inside = near(side, k)
-
-            @pl.when(inside & jnp.logical_not(exists(side)))
-            def _():
-                send_first(side, block).wait_recv()
-
-        def use(side, carry):
-            block = tp + (2 * side - 1) * k
-
-            @pl.when((block >= 0) & (block < tp_count))
-            def _():
-                project(block)
-                start_halo(block)
+
+        def settle(side, carry):
+            block, _ = near(side, k - 1)
+
+            inner = (block > 0) & (block < tp_count - 1) & ((k > 1) | (side == 0))
+            if slim:
+                inner = inner & (k == 1)
+
+            @pl.when(inner & plain)
+            def _():
+                attend(block)
 
             return carry
 
-        lax.fori_loop(0, 2, use, 0)
-
-        @pl.when(k == jnp.maximum(tp, tp_count - 1 - tp))
-        def _():
+        lax.fori_loop(0, 2, settle, 0)
+        return carry
+
+    lax.fori_loop(1, tp_count, first_hop, 0)
+    if assist:
+
+        @pl.when(ends)
+        def _():
+            def arrive(block):
+                @pl.when(block != tp)
+                def _():
+                    query_copy(block, toward(jnp.where(tp == 0, 0, 1))).wait_recv()
+                    kv_copy(block, toward(jnp.where(tp == 0, 0, 1))).wait_recv()
+                    start_halo(block)
+
+            each_part(arrive, tp_count)
             give_back(parts // 2, parts)
-
-        def settle(side, carry):
-            block = tp + (2 * side - 1) * (k - 1)
-
-            @pl.when((block > 0) & (block < tp_count - 1) & ((k > 1) | (side == 0)))
-            def _():
-                attend(block)
-
-            return carry
-
-        lax.fori_loop(0, 2, settle, 0)
-
-        if early:
-
-            @pl.when(k > 1)
-            def _():
-                reduce_step(2 * k)
-
-        return carry
-
-    lax.fori_loop(1, tp_count, first_hop, 0)
-
-    @pl.when(ep < ep_count - 1)
+            each_part(lambda block: attend(block + 1), tp_count - 2)
+
+    @pl.when(jnp.logical_not(helps) | (not slim))
     def _():
-        halo(1).wait_recv()
-
-    @pl.when(ep > 0)
-    def _():
-        halo(0).wait_recv()
-
-    def edge(side, carry):
-        attend((tp_count - 1) * (1 - side))
-        return carry
-
-    lax.fori_loop(0, 2, edge, 0)
+        each_part(lambda turn: edge(1 - turn), 2)
+
     own_weights = weights_of(tp)
 
     def last_part(part):
@@ -659,6 +855,9 @@
                 ref = gath2.at[block]
                 remote(ref, ref, s2.at[side, block], r2.at[block, 0], toward(side)).wait_send()
                 send_meta(side, block).wait_send()
+
+            @pl.when(carries(side) & passed)
+            def _():
                 send_first(side, block).wait_send()
 
             @pl.when(summed)
@@ -667,6 +866,27 @@
                     pass_on(side, block, part).wait_send()
 
     each_part(finish, tp_count)
+    if assist:
+
+        @pl.when(ends)
+        def _():
+            for copy in lend_out():
+                copy.wait_send()
+
+        @pl.when(helps)
+        def _():
+            for copies in relays() + (relays_across() if pair == 2 else []):
+                for copy in copies:
+                    copy.wait_send()
+
+            def sent(block):
+                @pl.when(block != tp + 1 - 2 * outward)
+                def _():
+                    query_copy(block, toward(outward)).wait_send()
+                    kv_copy(block, toward(outward)).wait_send()
+
+            each_part(sent, tp_count)
+
     each_part(lambda part: out_copy(part).wait())
     each_part(lambda block: mixed_copy(block).wait(), tp_count)
 
@@ -681,7 +901,7 @@
 
 def layer(
     second, first, gain_second, gain_first, router, routes, inverse, sink,
-    gate, up, down, sgate, sup, sdown, wq, wk, wv, ep_count, tp_count, slots,
+    gate, up, down, sgate, sup, sdown, wq, wk, wv, grp_count, ep_count, tp_count, slots,
 ):
     rows, width = second.shape
     experts = router.shape[0]
@@ -695,7 +915,7 @@
     span = tp_count * rows
     kv_cols = wk.shape[1] + wv.shape[1]
     return pl.pallas_call(
-        functools.partial(layer_kernel, ep_count, tp_count, slots),
+        functools.partial(layer_kernel, grp_count, ep_count, tp_count, slots),
         out_shape=(
             jax.ShapeDtypeStruct((rows, width), bf16),
             jax.ShapeDtypeStruct((span, wq.shape[1]), bf16),
@@ -722,6 +942,11 @@
             pltpu.VMEM(wq.shape, bf16),
             pltpu.VMEM(wk.shape, bf16),
             pltpu.VMEM(wv.shape, bf16),
+            pltpu.VMEM(wq.shape, bf16),
+            pltpu.VMEM(wk.shape, bf16),
+            pltpu.VMEM(wv.shape, bf16),
+            pltpu.VMEM((tp_count, rows, wq.shape[1]), bf16),
+            pltpu.VMEM((tp_count, rows, kv_cols), bf16),
             pltpu.VMEM((tp_count, rows, sgate.shape[1]), bf16),
             pltpu.VMEM((total, gate.shape[2]), bf16),
             pltpu.VMEM((span, LANES), f32),
@@ -745,6 +970,10 @@
             dma((2,)),
             dma((parts,)),
             dma((tp_count,)),
+            dma((2 * grp_count, grp_count, 3)),
+            dma((2 * grp_count, 3)),
+            dma((2, tp_count)),
+            dma((2, tp_count)),
         ],
         compiler_params=pltpu.CompilerParams(
             collective_id=0, has_side_effects=True, vmem_limit_bytes=VMEM_LIMIT
@@ -825,7 +1054,7 @@
         moe_in, mixer_in, moe_gain[None, :], mixer_gain[None, :], router.T, routes.T,
         jnp.asarray(np.tile(inverse, LANES // half)[None, :]), sink_logit[None, :],
         expert_gate, expert_up, expert_down, shared_gate, shared_up, shared_down,
-        w_query, w_key, w_value, ep_count, tp_count, slots,
+        w_query, w_key, w_value, lax.axis_size("grp"), ep_count, tp_count, slots,
     )
     moe_out, mixed = settle(moe_out, mixed)
     return (mixed, moe_out)

time: 91.2 us -> 88.1 us (0.966)
  the two profiles are of different devices: /device:TPU:1 before, /device:TPU:11 now
where the time goes in v4:
time: 88.1 us; the launch traced here: 87.9 us
  Pallas kernels  87.3 us (99%)
    pallas_call x1, Pallas kernels, layer(): pl.pallas_call(functools.partial(layer_kernel, grp_count, ep_count, tp_co...  85.4 us
    pallas_call x1, Pallas kernels, settle(): pl.pallas_call(settle_kernel, out_shape=(jax.ShapeDtypeStruct(first.shape...  1.89 us

profile of v4, /device:TPU:11, one launch (start us, length us, event | category | flops | bytes accessed | tf_op | source)
XLA Modules:
  0.0 87.9 jit_solution(3333550255531190310)
XLA Ops:
  0.6 85.4 %layer.1 = (bf16[128,2048]{1,0:T(8,128)(2,1)}, bf16[512,256]{1,0:T(8,128)(2,1)}) custom-call(bf16[128,2048]{1,0:T(8,128)(2,1)} %second_in.1, f32[1,2048]{1,0:T(1,128)} %bitcast.6, f32[1,2048]{1,0:T(1,128)} %bitcast.7, bf16[16,2048]{1,0:T(8,128)(2,1)} %bitcast.5, s32[4,128]{1,0:T(4,128)} %bitcast.8, f32[1,128]{1,0:T(1,128)} %constant.2.clone.inverse, ...), custom_call_target="tpu_custom_call" | custom-call | tf_op jit(solution)/shard_map/layer/pallas_call | solution.py:917
  86.0 1.9 %settle.1 = (bf16[128,2048]{1,0:T(8,128)(2,1)}, bf16[512,256]{1,0:T(8,128)(2,1)}) custom-call(bf16[128,2048]{1,0:T(8,128)(2,1)} %get-tuple-element.6.first, bf16[512,256]{1,0:T(8,128)(2,1)} %get-tuple-element.7.second), custom_call_target="tpu_custom_call" | custom-call | tf_op jit(solution)/shard_map/settle/pallas_call | solution.py:1012

commit v5 on v4

--- a/solution.py
+++ b/solution.py
@@ -15,7 +15,9 @@
 ROUTED_SCALE = 2.5
 LANES = 128
 CHUNK = 512
+PASS = 256
 LAG = 2
+AHEAD = 1
 MESH = pl.DeviceIdType.MESH
 VMEM_LIMIT = 63 * 2**20
 
@@ -55,10 +57,11 @@
 
 def layer_kernel(
     grp_count, ep_count, tp_count, slots,
-    second_in, gain_second, gain_first, router, routes, inverse, sink,
+    second_hbm, gain_second_hbm, router_hbm, routes_hbm, gain_first_hbm, inverse_hbm, sink_hbm,
     first_hbm, gate_hbm, up_hbm, down_hbm, sgate_hbm, sup_hbm, sdown_hbm, wq_hbm, wk_hbm, wv_hbm,
     out, mixed_out,
-    mixed, gath2, gath1, first_in, metag, sbuf, disp, back, sides, psend,
+    mixed, second_in, gain_second, router, routes, gain_first, inverse, sink,
+    gath2, gath1, first_in, metag, sbuf, disp, back, sides, psend,
     gate, up, down, sgate, sup, sdown, wq, wk, wv, far_q, far_k, far_v, lent_q, lent_kv,
     hidden, hexp, cosine, sine, qbuf, kvbuf,
     l_sem, s2, r2, sm, rm, s1, r1, sd, rd, sb, rb, sp, rs, hs, hr, out_sem, mixed_sem, ws, wr, qs, qr,
@@ -71,26 +74,31 @@
     f32, bf16 = jnp.float32, jnp.bfloat16
     away = pl.ds(slots, total - slots)
 
-    local = [
-        pltpu.make_async_copy(src, dst, l_sem.at[i])
-        for i, (src, dst) in enumerate(
-            [
-                (first_hbm, first_in),
-                (sgate_hbm, sgate),
-                (sup_hbm, sup),
-                (gate_hbm.at[0], gate),
-                (up_hbm.at[0], up),
-                (down_hbm.at[0], down),
-                (wq_hbm, wq),
-                (wk_hbm, wk),
-                (wv_hbm, wv),
-                (sdown_hbm, sdown),
-            ]
-        )
+    barrier = greet(grp, ep, tp, grp_count, ep_count, tp_count)
+    early_pairs = [
+        (second_hbm, second_in),
+        (gain_second_hbm, gain_second),
+        (routes_hbm, routes),
+        (router_hbm, router),
     ]
+    pairs = early_pairs + [
+        (gain_first_hbm, gain_first),
+        (first_hbm, first_in),
+        (sgate_hbm, sgate),
+        (sup_hbm, sup),
+        (wq_hbm, wq),
+        (wk_hbm, wk),
+        (wv_hbm, wv),
+        (inverse_hbm, inverse),
+        (sink_hbm, sink),
+        (gate_hbm.at[0], gate),
+        (up_hbm.at[0], up),
+        (down_hbm.at[0], down),
+        (sdown_hbm, sdown),
+    ]
+    local = [pltpu.make_async_copy(src, dst, l_sem.at[i]) for i, (src, dst) in enumerate(pairs)]
     for copy in local:
         copy.start()
-    barrier = greet(grp, ep, tp, grp_count, ep_count, tp_count)
 
     def toward(side):
         return (grp, ep, tp + 1 - 2 * side)
@@ -245,7 +253,7 @@
         return remote(sbuf.at[block, away], back.at[block, away], sb.at[block], rb.at[block, 0], peer(1))
 
     def pass_on(side, block, part):
-        span = part_span(part)
+        span = part_span(part, PASS)
         return remote(
             psend.at[block, :, span], sides.at[side, block, :, span],
             sp.at[block, part], rs.at[side, block, part], toward(side),
@@ -438,6 +446,8 @@
         mixed[pl.ds(base, rows), :] = jnp.concatenate(pieces, axis=1).astype(bf16)
         mixed_copy(block).start()
 
+    for copy in local[: len(early_pairs)]:
+        copy.wait()
     normalize(second_in, gain_second, gath2.at[tp])
     ids = lax.broadcasted_iota(jnp.int32, (experts, rows), 0)
     hit = ids == routes[0:1, :]
@@ -456,7 +466,7 @@
     def send_own(part):
         for side in range(2):
 
-            @pl.when(exists(side) & jnp.logical_not(late(side)))
+            @pl.when(exists(side) & (jnp.logical_not(late(side)) | (part < AHEAD)))
             def _():
                 send_second(side, tp, part).start()
 
@@ -481,7 +491,8 @@
         return carry
 
     lax.fori_loop(1, parts, pick_rest, 0)
-    local[0].wait()
+    for copy in local[len(early_pairs) : len(early_pairs) + 2]:
+        copy.wait()
     normalize(first_in, gain_first, gath1.at[tp])
 
     @pl.when(tp == 0)
@@ -500,7 +511,7 @@
     def _():
         kvbuf[(tp_count + 1) * rows : (tp_count + 2) * rows, :] = jnp.zeros((rows, kvbuf.shape[1]), bf16)
 
-    for copy in local[1:]:
+    for copy in local[len(early_pairs) + 2 :]:
         copy.wait()
     if assist:
 
@@ -536,12 +547,17 @@
         return_part(block, part).wait_recv()
         own = value_of(block, weights, span)
 
-        @pl.when(exists(1 - side))
-        def _():
-            pass_on(side, block, part).wait_recv()
-
-        psend[block, :, span] = (own + sides[side, block, :, span].astype(f32)).astype(bf16)
-        pass_on(side, block, part).start()
+        for i in range(CHUNK // PASS):
+            number = part * (CHUNK // PASS) + i
+            piece = part_span(number, PASS)
+
+            @pl.when(exists(1 - side))
+            def _():
+                pass_on(side, block, number).wait_recv()
+
+            part_sum = own[:, i * PASS : (i + 1) * PASS] + sides[side, block, :, piece].astype(f32)
+            psend[block, :, piece] = part_sum.astype(bf16)
+            pass_on(side, block, number).start()
 
     def edge(last):
         @pl.when((last == 1) & (ep < ep_count - 1))
@@ -553,6 +569,11 @@
             halo(0).wait_recv()
 
         attend((tp_count - 1) * last)
+
+    def give_back(low, high):
+        for part in range(low, high):
+            for d in range(1, ep_count):
+                return_copy(tp, d, part).start()
 
     def reduce_merged():
         end = (tp_count - 1) * (1 - outward)
@@ -572,13 +593,22 @@
 
             lax.fori_loop(0, 3, stream, 0)
 
-            @pl.when(i == 0)
+            @pl.when(i == 1)
+            def _():
+                block, _ = near(outward, 2)
+                send_first(outward, block).wait_recv()
+                project_far(block)
+                project(block)
+                start_halo(block)
+                give_back(0, parts)
+
+            @pl.when(i == 2)
             def _():
                 attend(second)
 
             @pl.when((i == 3) | (i == 5))
             def _():
-                edge(jnp.where(i == 3, 1, 0))
+                edge(jnp.where(i == 3, outward, 1 - outward))
 
         each_part(slot, parts + 2 * LAG)
 
@@ -627,7 +657,7 @@
 
                     @pl.when(late(side) & (k == 1) & (part == parts - 1))
                     def _():
-                        for own in range(parts):
+                        for own in range(AHEAD, parts):
                             send_second(side, tp, own).start()
 
                     pick_part(block, part)
@@ -653,11 +683,6 @@
                 def _():
                     reduce_step(1)
 
-            if assist:
-
-                @pl.when(helps & (k == 2) & (turn == LAG + 1))
-                def _():
-                    relay_first()
 
             middle = ends & (k > 1) & (k == tp_count - 1) & (turn == LAG)
 
@@ -674,6 +699,12 @@
             @pl.when(inside)
             def _():
                 shared_hidden(block)
+
+        if assist:
+
+            @pl.when(helps & (k == 2))
+            def _():
+                relay_first()
 
         if slim:
 
@@ -698,11 +729,6 @@
 
     experts_at(tp_count - 1)
 
-    def give_back(low, high):
-        for part in range(low, high):
-            for d in range(1, ep_count):
-                return_copy(tp, d, part).start()
-
     @pl.when(ends | (not slim))
     def _():
         give_back(0, parts // 2)
@@ -718,7 +744,7 @@
         def open_at(side):
             block, inside = near(side, k)
             if slim:
-                inside = inside & ((k > 1) | (side == outward))
+                inside = inside & (k == 1) & (side == outward)
             return block, inside
 
         for side in range(2):
@@ -743,6 +769,9 @@
                 def one(turn, carry):
                     block, inside = near(outward, k * turn)
 
+                    if slim:
+                        inside = inside & (k == 1)
+
                     @pl.when(inside & ((turn == 1) | (k == 1)))
                     def _():
                         project_far(block)
@@ -762,9 +791,11 @@
             return carry
 
         lax.fori_loop(0, 2, use, 0)
-        @pl.when((k == jnp.maximum(tp, tp_count - 1 - tp)) & plain)
-        def _():
-            give_back(0 if slim else parts // 2, parts)
+        if not slim:
+
+            @pl.when((k == jnp.maximum(tp, tp_count - 1 - tp)) & plain)
+            def _():
+                give_back(parts // 2, parts)
 
         if slim:
 
@@ -820,7 +851,7 @@
 
     @pl.when(jnp.logical_not(helps) | (not slim))
     def _():
-        each_part(lambda turn: edge(1 - turn), 2)
+        each_part(lambda turn: edge(jnp.where(2 * tp < tp_count, 1 - turn, turn)), 2)
 
     own_weights = weights_of(tp)
 
@@ -829,13 +860,15 @@
         return_part(tp, part).wait_recv()
         own = value_of(tp, own_weights, span)
 
-        @pl.when(tp > 0)
-        def _():
-            pass_on(0, tp, part).wait_recv()
-
-        @pl.when(tp < tp_count - 1)
-        def _():
-            pass_on(1, tp, part).wait_recv()
+        for i in range(CHUNK // PASS):
+
+            @pl.when(tp > 0)
+            def _():
+                pass_on(0, tp, part * (CHUNK // PASS) + i).wait_recv()
+
+            @pl.when(tp < tp_count - 1)
+            def _():
+                pass_on(1, tp, part * (CHUNK // PASS) + i).wait_recv()
 
         psend[tp, :, span] = (
             own + sides[0, tp, :, span].astype(f32) + sides[1, tp, :, span].astype(f32)
@@ -862,8 +895,8 @@
 
             @pl.when(summed)
             def _():
-                for part in range(parts):
-                    pass_on(side, block, part).wait_send()
+                for number in range(width // PASS):
+                    pass_on(side, block, number).wait_send()
 
     each_part(finish, tp_count)
     if assist:
@@ -905,8 +938,6 @@
 ):
     rows, width = second.shape
     experts = router.shape[0]
-    vmem = pl.BlockSpec(memory_space=pltpu.VMEM)
-    smem = pl.BlockSpec(memory_space=pltpu.SMEM)
     hbm = pl.BlockSpec(memory_space=pl.ANY)
     dma = pltpu.SemaphoreType.DMA
     bf16, f32 = jnp.bfloat16, jnp.float32
@@ -920,10 +951,17 @@
             jax.ShapeDtypeStruct((rows, width), bf16),
             jax.ShapeDtypeStruct((span, wq.shape[1]), bf16),
         ),
-        in_specs=[vmem] * 6 + [smem] + [hbm] * 10,
+        in_specs=[hbm] * 17,
         out_specs=(hbm, hbm),
         scratch_shapes=[
             pltpu.VMEM((span, wq.shape[1]), bf16),
+            pltpu.VMEM((rows, width), bf16),
+            pltpu.VMEM(gain_second.shape, f32),
+            pltpu.VMEM(router.shape, bf16),
+            pltpu.VMEM(routes.shape, jnp.int32),
+            pltpu.VMEM(gain_first.shape, f32),
+            pltpu.VMEM(inverse.shape, f32),
+            pltpu.SMEM(sink.shape, f32),
             pltpu.VMEM((tp_count, rows, width), bf16),
             pltpu.VMEM((tp_count, rows, width), bf16),
             pltpu.VMEM((rows, width), bf16),
@@ -953,7 +991,7 @@
             pltpu.VMEM((span, LANES), f32),
             pltpu.VMEM((span, wq.shape[1]), bf16),
             pltpu.VMEM((span + 2 * rows, kv_cols), bf16),
-            dma((10,)),
+            dma((17,)),
             dma((2, tp_count)),
             dma((tp_count, parts)),
             dma((2, tp_count)),
@@ -964,8 +1002,8 @@
             dma((tp_count,)),
             dma((tp_count,)),
             dma((tp_count, parts)),
-            dma((tp_count, parts)),
-            dma((2, tp_count, parts)),
+            dma((tp_count, width // PASS)),
+            dma((2, tp_count, width // PASS)),
             dma((2,)),
             dma((2,)),
             dma((parts,)),
@@ -980,7 +1018,7 @@
         ),
         name="layer",
     )(
-        second, gain_second, gain_first, router, routes, inverse, sink,
+        second, gain_second, router, routes, gain_first, inverse, sink,
         first, gate, up, down, sgate, sup, sdown, wq, wk, wv,
     )
 

time: 88.1 us -> 84.8 us (0.963)
  the two profiles are of different devices: /device:TPU:11 before, /device:TPU:1 now
where the time goes in v5:
time: 84.8 us; the launch traced here: 83.2 us
  Pallas kernels  82.4 us (97%)
    pallas_call x1, Pallas kernels, layer(): pl.pallas_call(functools.partial(layer_kernel, grp_count, ep_count, tp_co...  80.5 us
    pallas_call x1, Pallas kernels, settle(): pl.pallas_call(settle_kernel, out_shape=(jax.ShapeDtypeStruct(first.shape...  1.89 us

profile of v5, /device:TPU:1, one launch (start us, length us, event | category | flops | bytes accessed | tf_op | source)
XLA Modules:
  0.0 83.2 jit_solution(12359497409644767809)
XLA Ops:
  0.6 80.5 %layer.1 = (bf16[128,2048]{1,0:T(8,128)(2,1)}, bf16[512,256]{1,0:T(8,128)(2,1)}) custom-call(bf16[128,2048]{1,0:T(8,128)(2,1)} %second_hbm.1, f32[1,2048]{1,0:T(1,128)} %bitcast.6, bf16[16,2048]{1,0:T(8,128)(2,1)} %bitcast.5, s32[4,128]{1,0:T(4,128)} %bitcast.8, f32[1,2048]{1,0:T(1,128)} %bitcast.7, f32[1,128]{1,0:T(1,128)} %constant.2.clone.inverse_hbm, ...), custom_call_target="tpu_custom_call" | custom-call | tf_op jit(solution)/shard_map/layer/pallas_call | solution.py:948
  81.1 1.9 %settle.1 = (bf16[128,2048]{1,0:T(8,128)(2,1)}, bf16[512,256]{1,0:T(8,128)(2,1)}) custom-call(bf16[128,2048]{1,0:T(8,128)(2,1)} %get-tuple-element.6.first, bf16[512,256]{1,0:T(8,128)(2,1)} %get-tuple-element.7.second), custom_call_target="tpu_custom_call" | custom-call | tf_op jit(solution)/shard_map/settle/pallas_call | solution.py:1050

commit v6 on v5

--- a/solution.py
+++ b/solution.py
@@ -139,12 +139,15 @@
     def late(side):
         return (tp == 1 + side * (tp_count - 3)) & swaps
 
+    def lane(side, block, owner):
+        return jnp.where((block == owner) & (side == 1), tp_count, block)
+
     def send_second(side, block, part):
         ref = gath2.at[block, :, part_span(part)]
-        return remote(ref, ref, s2.at[side, block], r2.at[block, part], toward(side))
+        return remote(ref, ref, s2.at[lane(side, block, tp)], r2.at[block, part], toward(side))
 
     def send_meta(side, block):
-        return remote(metag.at[block], metag.at[block], sm.at[side, block], rm.at[block], toward(side))
+        return remote(metag.at[block], metag.at[block], sm.at[lane(side, block, tp)], rm.at[block], toward(side))
 
     assist = tp_count >= 4
     ends = (tp == 0) | (tp == tp_count - 1)
@@ -169,7 +172,7 @@
         return [
             remote(
                 (near_ref if own else far_ref).at[span], far_ref.at[span],
-                ws.at[share, to, i], wr.at[share, i], device,
+                ws.at[to, i], wr.at[share, i], device,
             )
             for i, (near_ref, far_ref) in enumerate(lent)
         ]
@@ -192,7 +195,7 @@
     def relays_across():
         copies = []
         for d in range(1, grp_count):
-            copies.append(lend(share_of(lax.rem(grp + d, grp_count), core), 0, partner(), False))
+            copies.append(lend(share_of(lax.rem(grp + d, grp_count), core), grp_count - 1 + d, partner(), False))
         return copies
 
     def relay_first():
@@ -218,16 +221,22 @@
 
     def query_copy(block, device):
         return remote(
-            lent_q.at[block], qbuf.at[part_span(block, rows)], qs.at[0, block], qr.at[0, block], device
+            lent_q.at[block], qbuf.at[part_span(block, rows)], qs.at[0], qr.at[0], device
         )
 
     def kv_copy(block, device):
         return remote(
-            lent_kv.at[block], kvbuf.at[part_span(block + 1, rows)], qs.at[1, block], qr.at[1, block], device
+            lent_kv.at[block], kvbuf.at[part_span(block + 1, rows)], qs.at[1], qr.at[1], device
         )
 
+    def lent_all(device):
+        span = pl.ds(0, (tp_count - 1) * rows)
+        return [
+            remote(ref.at[span], ref.at[span], qs.at[i], qr.at[i], device) for i, ref in enumerate((qbuf, kvbuf))
+        ]
+
     def send_first(side, block):
-        return remote(gath1.at[block], gath1.at[block], s1.at[side, block], r1.at[block], toward(side))
+        return remote(gath1.at[block], gath1.at[block], s1.at[lane(side, block, tp)], r1.at[block], toward(side))
 
     def dispatch_copy(block, d, span):
         mine = pl.ds(d * slots, slots)
@@ -252,11 +261,11 @@
     def return_all(block):
         return remote(sbuf.at[block, away], back.at[block, away], sb.at[block], rb.at[block, 0], peer(1))
 
-    def pass_on(side, block, part):
+    def pass_on(side, block, part, owner):
         span = part_span(part, PASS)
         return remote(
             psend.at[block, :, span], sides.at[side, block, :, span],
-            sp.at[block, part], rs.at[side, block, part], toward(side),
+            sp.at[block], rs.at[lane(side, block, owner), part], toward(side),
         )
 
     def halo(side):
@@ -269,11 +278,11 @@
 
     def out_copy(part):
         span = part_span(part)
-        return pltpu.make_async_copy(psend.at[tp, :, span], out.at[:, span], out_sem.at[part])
+        return pltpu.make_async_copy(psend.at[tp, :, span], out.at[:, span], out_sem.at[0])
 
     def mixed_copy(block):
         span = part_span(block, rows)
-        return pltpu.make_async_copy(mixed.at[span], mixed_out.at[span], mixed_sem.at[block])
+        return pltpu.make_async_copy(mixed.at[span], mixed_out.at[span], mixed_sem.at[0])
 
     def normalize(source, gain, target):
         def squares(part, carry):
@@ -553,11 +562,11 @@
 
             @pl.when(exists(1 - side))
             def _():
-                pass_on(side, block, number).wait_recv()
+                pass_on(side, block, number, tp).wait_recv()
 
             part_sum = own[:, i * PASS : (i + 1) * PASS] + sides[side, block, :, piece].astype(f32)
             psend[block, :, piece] = part_sum.astype(bf16)
-            pass_on(side, block, number).start()
+            pass_on(side, block, number, tp + 1 - 2 * side).start()
 
     def edge(last):
         @pl.when((last == 1) & (ep < ep_count - 1))
@@ -838,14 +847,9 @@
 
         @pl.when(ends)
         def _():
-            def arrive(block):
-                @pl.when(block != tp)
-                def _():
-                    query_copy(block, toward(jnp.where(tp == 0, 0, 1))).wait_recv()
-                    kv_copy(block, toward(jnp.where(tp == 0, 0, 1))).wait_recv()
-                    start_halo(block)
-
-            each_part(arrive, tp_count)
+            for copy in lent_all(toward(jnp.where(tp == 0, 0, 1))):
+                copy.wait_recv()
+            start_halo(tp_count - 1 - tp)
             give_back(parts // 2, parts)
             each_part(lambda block: attend(block + 1), tp_count - 2)
 
@@ -864,11 +868,11 @@
 
             @pl.when(tp > 0)
             def _():
-                pass_on(0, tp, part * (CHUNK // PASS) + i).wait_recv()
+                pass_on(0, tp, part * (CHUNK // PASS) + i, tp).wait_recv()
 
             @pl.when(tp < tp_count - 1)
             def _():
-                pass_on(1, tp, part * (CHUNK // PASS) + i).wait_recv()
+                pass_on(1, tp, part * (CHUNK // PASS) + i, tp).wait_recv()
 
         psend[tp, :, span] = (
             own + sides[0, tp, :, span].astype(f32) + sides[1, tp, :, span].astype(f32)
@@ -886,7 +890,7 @@
             @pl.when(exists(side) & passed)
             def _():
                 ref = gath2.at[block]
-                remote(ref, ref, s2.at[side, block], r2.at[block, 0], toward(side)).wait_send()
+                remote(ref, ref, s2.at[lane(side, block, tp)], r2.at[block, 0], toward(side)).wait_send()
                 send_meta(side, block).wait_send()
 
             @pl.when(carries(side) & passed)
@@ -895,8 +899,9 @@
 
             @pl.when(summed)
             def _():
-                for number in range(width // PASS):
-                    pass_on(side, block, number).wait_send()
+                remote(
+                    psend.at[block], sides.at[side, block], sp.at[block], rs.at[block, 0], toward(side)
+                ).wait_send()
 
     each_part(finish, tp_count)
     if assist:
@@ -912,16 +917,12 @@
                 for copy in copies:
                     copy.wait_send()
 
-            def sent(block):
-                @pl.when(block != tp + 1 - 2 * outward)
-                def _():
-                    query_copy(block, toward(outward)).wait_send()
-                    kv_copy(block, toward(outward)).wait_send()
-
-            each_part(sent, tp_count)
-
-    each_part(lambda part: out_copy(part).wait())
-    each_part(lambda block: mixed_copy(block).wait(), tp_count)
+            for copy in lent_all(toward(outward)):
+                copy.wait_send()
+
+
+    pltpu.make_async_copy(mixed, mixed_out, mixed_sem.at[0]).wait()
+    pltpu.make_async_copy(psend.at[tp], out, out_sem.at[0]).wait()
 
     @pl.when(ep < ep_count - 1)
     def _():
@@ -992,26 +993,26 @@
             pltpu.VMEM((span, wq.shape[1]), bf16),
             pltpu.VMEM((span + 2 * rows, kv_cols), bf16),
             dma((17,)),
-            dma((2, tp_count)),
+            dma((tp_count + 1,)),
             dma((tp_count, parts)),
-            dma((2, tp_count)),
+            dma((tp_count + 1,)),
             dma((tp_count,)),
-            dma((2, tp_count)),
+            dma((tp_count + 1,)),
             dma((tp_count,)),
             dma((tp_count,)),
             dma((tp_count,)),
             dma((tp_count,)),
             dma((tp_count, parts)),
-            dma((tp_count, width // PASS)),
-            dma((2, tp_count, width // PASS)),
+            dma((tp_count,)),
+            dma((tp_count + 1, width // PASS)),
             dma((2,)),
             dma((2,)),
-            dma((parts,)),
-            dma((tp_count,)),
-            dma((2 * grp_count, grp_count, 3)),
+            dma((1,)),
+            dma((1,)),
+            dma((2 * grp_count - 1, 3)),
             dma((2 * grp_count, 3)),
-            dma((2, tp_count)),
-            dma((2, tp_count)),
+            dma((2,)),
+            dma((2,)),
         ],
         compiler_params=pltpu.CompilerParams(
             collective_id=0, has_side_effects=True, vmem_limit_bytes=VMEM_LIMIT

time: 84.8 us -> 83.9 us (0.989)
  Pallas kernels: 82.4 us -> 81.5 us
    pallas_call x1, Pallas kernels: 80.5 us -> 79.6 us  [layer(): pl.pallas_call(functools.partial(layer_kernel, grp_count, ep_count, tp_co...]
where the time goes in v6:
time: 83.9 us; the launch traced here: 82.3 us
  Pallas kernels  81.5 us (97%)
    pallas_call x1, Pallas kernels, layer(): pl.pallas_call(functools.partial(layer_kernel, grp_count, ep_count, tp_co...  79.6 us
    pallas_call x1, Pallas kernels, settle(): pl.pallas_call(settle_kernel, out_shape=(jax.ShapeDtypeStruct(first.shape...  1.89 us

profile of v6, /device:TPU:1, one launch (start us, length us, event | category | flops | bytes accessed | tf_op | source)
XLA Modules:
  0.0 82.3 jit_solution(10892247724138083289)
XLA Ops:
  0.6 79.6 %layer.1 = (bf16[128,2048]{1,0:T(8,128)(2,1)}, bf16[512,256]{1,0:T(8,128)(2,1)}) custom-call(bf16[128,2048]{1,0:T(8,128)(2,1)} %second_hbm.1, f32[1,2048]{1,0:T(1,128)} %bitcast.6, bf16[16,2048]{1,0:T(8,128)(2,1)} %bitcast.5, s32[4,128]{1,0:T(4,128)} %bitcast.8, f32[1,2048]{1,0:T(1,128)} %bitcast.7, f32[1,128]{1,0:T(1,128)} %constant.2.clone.inverse_hbm, ...), custom_call_target="tpu_custom_call" | custom-call | tf_op jit(solution)/shard_map/layer/pallas_call | solution.py:949
  80.3 1.9 %settle.1 = (bf16[128,2048]{1,0:T(8,128)(2,1)}, bf16[512,256]{1,0:T(8,128)(2,1)}) custom-call(bf16[128,2048]{1,0:T(8,128)(2,1)} %get-tuple-element.6.first, bf16[512,256]{1,0:T(8,128)(2,1)} %get-tuple-element.7.second), custom_call_target="tpu_custom_call" | custom-call | tf_op jit(solution)/shard_map/settle/pallas_call | solution.py:1051

commit v7 on v6

--- a/solution.py
+++ b/solution.py
@@ -17,7 +17,7 @@
 CHUNK = 512
 PASS = 256
 LAG = 2
-AHEAD = 1
+AHEAD = 2
 MESH = pl.DeviceIdType.MESH
 VMEM_LIMIT = 63 * 2**20
 
@@ -621,6 +621,30 @@
 
         each_part(slot, parts + 2 * LAG)
 
+    def arrive():
+        for copy in lent_all(toward(jnp.where(tp == 0, 0, 1))):
+            copy.wait_recv()
+        start_halo(tp_count - 1 - tp)
+
+    def reduce_ends():
+        side = jnp.where(tp == 0, 0, 1)
+        block = jnp.where(tp == 0, tp_count - 2, 1)
+        weights = weights_of(block)
+
+        def one(part):
+            reduce_piece(side, block, part, weights)
+
+            @pl.when(part == 0)
+            def _():
+                arrive()
+                give_back(parts // 2, parts)
+
+            @pl.when(part < tp_count - 2)
+            def _():
+                attend(part + 1)
+
+        each_part(one)
+
     def reduce_step(step):
         def one(turn, carry):
             side = jnp.where(2 * tp < tp_count, 1 - turn, turn)
@@ -688,12 +712,12 @@
 
             if early:
 
-                @pl.when(ends & (k == tp_count - 1) & (turn == LAG + 1))
+                @pl.when(ends & (k == tp_count - 1) & (turn == LAG + 2))
                 def _():
                     reduce_step(1)
 
 
-            middle = ends & (k > 1) & (k == tp_count - 1) & (turn == LAG)
+            middle = ends & (k > 1) & (k == tp_count - 1) & (turn == LAG + 1)
 
             @pl.when(middle | ((k == 1) & (turn == LAG + 2)))
             def _():
@@ -810,7 +834,7 @@
 
             @pl.when((k == 2) & ends)
             def _():
-                reduce_step(3)
+                reduce_ends()
 
             @pl.when((k == 2) & helps)
             def _():
@@ -847,11 +871,10 @@
 
         @pl.when(ends)
         def _():
-            for copy in lent_all(toward(jnp.where(tp == 0, 0, 1))):
-                copy.wait_recv()
-            start_halo(tp_count - 1 - tp)
-            give_back(parts // 2, parts)
-            each_part(lambda block: attend(block + 1), tp_count - 2)
+            if not slim:
+                arrive()
+                give_back(parts // 2, parts)
+                each_part(lambda block: attend(block + 1), tp_count - 2)
 
     @pl.when(jnp.logical_not(helps) | (not slim))
     def _():

time: 83.9 us -> 83.7 us (level)
  no operation moved by 1% of the time
where the time goes in v7:
time: 83.7 us; the launch traced here: 82.1 us
  Pallas kernels  81.5 us (97%)
    pallas_call x1, Pallas kernels, layer(): pl.pallas_call(functools.partial(layer_kernel, grp_count, ep_count, tp_co...  79.6 us
    pallas_call x1, Pallas kernels, settle(): pl.pallas_call(settle_kernel, out_shape=(jax.ShapeDtypeStruct(first.shape...  1.89 us

profile of v7, /device:TPU:1, one launch (start us, length us, event | category | flops | bytes accessed | tf_op | source)
XLA Modules:
  0.0 82.1 jit_solution(4521396594294956118)
XLA Ops:
  0.6 79.6 %layer.1 = (bf16[128,2048]{1,0:T(8,128)(2,1)}, bf16[512,256]{1,0:T(8,128)(2,1)}) custom-call(bf16[128,2048]{1,0:T(8,128)(2,1)} %second_hbm.1, f32[1,2048]{1,0:T(1,128)} %bitcast.6, bf16[16,2048]{1,0:T(8,128)(2,1)} %bitcast.5, s32[4,128]{1,0:T(4,128)} %bitcast.8, f32[1,2048]{1,0:T(1,128)} %bitcast.7, f32[1,128]{1,0:T(1,128)} %constant.2.clone.inverse_hbm, ...), custom_call_target="tpu_custom_call" | custom-call | tf_op jit(solution)/shard_map/layer/pallas_call | solution.py:972
  80.2 1.9 %settle.1 = (bf16[128,2048]{1,0:T(8,128)(2,1)}, bf16[512,256]{1,0:T(8,128)(2,1)}) custom-call(bf16[128,2048]{1,0:T(8,128)(2,1)} %get-tuple-element.6.first, bf16[512,256]{1,0:T(8,128)(2,1)} %get-tuple-element.7.second), custom_call_target="tpu_custom_call" | custom-call | tf_op jit(solution)/shard_map/settle/pallas_call | solution.py:1074
